TPU v7x, 128 devices: a whole 4x4x4 slice. The times are simulated.
128 devices in a mesh: sp: 16 (over z, y), tp: 8 (over x, core).
Axes of the slice: x: 4, y: 4, z: 4, core: 2. Of those that a mesh axis runs over, the one named last changes fastest.
Arguments:
- resid: bfloat16 [16384, 2048], P(('sp', 'tp')), may hold values from -6 to 6
- queries: bfloat16 [16384, 2048], P('sp', 'tp'), may hold values from -6 to 6
- keys: bfloat16 [16384, 2048], P('sp', 'tp'), may hold values from -6 to 6
- values: bfloat16 [16384, 4096], P('sp', 'tp'), may hold values from -6 to 6
- gates: bfloat16 [16384, 4096], P('sp', 'tp'), may hold values from -6 to 6
- log_decay: float32 [8, 16384], P('tp', 'sp'), may hold values from -1 to 0
- retention_output_weight: bfloat16 [4096, 2048], P('tp'), may hold values from -0.125 to 0.125
- norm_gain: bfloat16 [2048], replicated, may hold values from 0.099609375 to 1.8984375
- up_weight: bfloat16 [2048, 8192], P('sp', 'tp'), may hold values from -0.125 to 0.125
- down_weight: bfloat16 [8192, 2048], P('tp', 'sp'), may hold values from -0.0625 to 0.0625
Outputs:
- layer_out: bfloat16 [16384, 2048], P(('sp', 'tp'))
All inputs are finite; a program needn't handle non-finite values.
Results may differ from a plain program's by a relative error of at most 0.02.
Values may be sent and summed in bfloat16 or wider, within the bound.
A program may use at most 128 MiB of HBM per device.

v0:
```python
import jax
import jax.numpy as jnp
from jax import lax
from jax.sharding import Mesh
from jax.sharding import PartitionSpec as P

DK = 256
DV = 512
BLOCK = 128
SP = ("sp_0", "sp_1")
SP_TP = ("sp_0", "sp_1", "tp")


tiny_stabilizer = 1e-06


def neutral_like(value, identity):
    return jax.tree.map(
        lambda part, zero: jnp.zeros_like(part) + jnp.asarray(zero, part.dtype), value, identity
    )


def carried_in(value, axes, combine, identity):
    before = start = neutral_like(value, identity)
    total = value
    for axis in reversed(axes):
        length, position = (lax.axis_size(axis), lax.axis_index(axis))
        pieces = jax.tree.map(
            lambda part, kind: lax.all_gather(part.astype(kind), axis),
            total,
            (jnp.bfloat16, jnp.bfloat16),
        )
        inside, total = (start, start)
        for k in range(length):
            passed = k < position
            total = combine(
                total, jax.tree.map(lambda part, own: part[k].astype(own.dtype), pieces, value)
            )
            inside = jax.tree.map(lambda new, old: jnp.where(passed, new, old), total, inside)
        before = combine(inside, before)
    return before


def in_order(tiles, dim):
    tiles = jnp.moveaxis(tiles, 0, dim)
    shape = tiles.shape
    return tiles.reshape(*shape[:dim], shape[dim] * shape[dim + 1], *shape[dim + 2 :])


def gather_packed(arrays, axis, dims):
    flat = jnp.concatenate([a.reshape(-1) for a in arrays])
    lines, at, gathered = (lax.all_gather(flat, axis), 0, [])
    for a, dim in zip(arrays, dims):
        tiles = lines[:, at : at + a.size].reshape(-1, *a.shape)
        gathered.append(in_order(tiles, dim))
        at += a.size
    return tuple(gathered)


def cut_along(value, dim, length):
    shape = value.shape
    tiles = value.reshape(*shape[:dim], length, shape[dim] // length, *shape[dim + 1 :])
    return jnp.moveaxis(tiles, dim, 0)


def summed_on_arrival(value, axis, dim):
    tiles = cut_along(value, dim, lax.axis_size(axis))
    arrived = lax.all_to_all(tiles, axis, split_axis=0, concat_axis=0, tiled=True)
    return arrived.astype(jnp.float32).sum(axis=0)


def rotate(values_in, token_indices):
    half_width = values_in.shape[-1] // 2
    inverse = 10000.0 ** (-jnp.arange(0, 2 * half_width, 2, dtype=jnp.float32) / (2 * half_width))
    angles = token_indices[:, None].astype(jnp.float32) * inverse[None, :]
    cosine = jnp.cos(angles)[:, None, :]
    sine_lookup = jnp.sin(angles)[:, None, :]
    first_half = values_in[..., :half_width]
    second = values_in[..., half_width:]
    return jnp.concatenate(
        [first_half * cosine - second * sine_lookup, first_half * sine_lookup + second * cosine],
        axis=-1,
    )


def normalize(updated, norm_gain):
    widened = updated.astype(jnp.float32)
    scaled = widened * lax.rsqrt(
        jnp.mean(widened * widened, axis=-1, keepdims=True) + tiny_stabilizer
    )
    return (scaled * norm_gain.astype(jnp.float32)).astype(jnp.bfloat16)


def activate(preact):
    positive = jnp.maximum(preact, 0.0)
    return (positive * positive).astype(jnp.bfloat16)


def combine(earlier, later):
    return (earlier[0] * later[0], later[0][:, None, None] * earlier[1] + later[1])


def carry_step(prior, inputs):
    term, decay = inputs
    return (decay[:, None, None] * prior + term, prior)


def retention(queries, keys, values, gates, log_decay):
    row_count = queries.shape[0]
    local_heads = log_decay.shape[0]
    blocks = row_count // BLOCK
    token_indices = lax.axis_index(SP) * row_count + jnp.arange(row_count, dtype=jnp.int32)
    query_rot = rotate(
        queries.reshape(row_count, local_heads, DK).astype(jnp.float32), token_indices
    )
    query_rot = query_rot.astype(jnp.bfloat16).reshape(blocks, BLOCK, local_heads, DK)
    key_rot = rotate(
        keys.reshape(row_count, local_heads, DK).astype(jnp.float32), token_indices
    ) * DK ** (-0.5)
    key_rot = key_rot.astype(jnp.bfloat16).reshape(blocks, BLOCK, local_heads, DK)
    value_blk = values.reshape(blocks, BLOCK, local_heads, DV)
    gate_blk = gates.reshape(blocks, BLOCK, local_heads, DV)
    cumulative = jnp.cumsum(log_decay.reshape(local_heads, blocks, BLOCK), axis=2)
    causal = jnp.arange(BLOCK)[:, None] >= jnp.arange(BLOCK)[None, :]
    spread = cumulative[:, :, :, None] - cumulative[:, :, None, :]
    factor = jnp.where(causal, jnp.exp(jnp.minimum(spread, 0.0)), 0.0)
    scores = jnp.einsum("nihd,njhd->hnij", query_rot, key_rot, preferred_element_type=jnp.float32)
    weights = (scores * factor).astype(jnp.bfloat16)
    within_block = jnp.einsum(
        "hnij,njhv->nihv", weights, value_blk, preferred_element_type=jnp.float32
    )
    tile_count_all = cumulative[:, :, -1]
    to_end = jnp.transpose(jnp.exp(tile_count_all[:, :, None] - cumulative), (1, 2, 0))[..., None]
    key_decayed = (key_rot * to_end).astype(jnp.bfloat16)
    block_terms = jnp.einsum(
        "njhd,njhv->nhdv", key_decayed, value_blk, preferred_element_type=jnp.float32
    )
    local_state, from_local = lax.scan(
        carry_step,
        jnp.zeros((local_heads, DK, DV), jnp.float32),
        (block_terms, jnp.exp(tile_count_all).T),
    )
    device_decay = jnp.exp(jnp.sum(tile_count_all, axis=1))
    identity = (
        jnp.ones((local_heads,), jnp.float32),
        jnp.zeros((local_heads, DK, DV), jnp.float32),
    )
    unused, incoming = carried_in((device_decay, local_state), SP, combine, identity)
    before = jnp.exp(jnp.cumsum(tile_count_all, axis=1) - tile_count_all).T
    states = (before[:, :, None, None] * incoming[None] + from_local).astype(jnp.bfloat16)
    from_start = jnp.transpose(jnp.exp(cumulative), (1, 2, 0))[..., None]
    query_decayed = (query_rot * from_start).astype(jnp.bfloat16)
    carried_part = jnp.einsum(
        "nihd,nhdv->nihv", query_decayed, states, preferred_element_type=jnp.float32
    )
    retained = within_block + carried_part
    normed = retained * lax.rsqrt(
        jnp.mean(retained * retained, axis=-1, keepdims=True) + tiny_stabilizer
    )
    gated_out = (jax.nn.silu(gate_blk.astype(jnp.float32)) * normed).astype(jnp.bfloat16)
    return gated_out.reshape(row_count, local_heads * DV)


def body(
    resid,
    queries,
    keys,
    values,
    gates,
    log_decay,
    retention_output_weight,
    norm_gain,
    up_weight,
    down_weight,
):
    up_whole, down_whole = gather_packed((up_weight, down_weight), SP, (0, 1))
    gated_out = retention(queries, keys, values, gates, log_decay)
    selected = gated_out
    mixed_sum = lax.psum_scatter(
        jnp.dot(selected, retention_output_weight, preferred_element_type=jnp.float32).astype(
            jnp.bfloat16
        ),
        "tp",
        scatter_dimension=0,
        tiled=True,
    ).astype(jnp.float32)
    updated = (resid.astype(jnp.float32) + mixed_sum).astype(jnp.bfloat16)
    normed_whole = lax.all_gather(normalize(updated, norm_gain), "tp", axis=0, tiled=True)
    hidden = activate(jnp.dot(normed_whole, up_whole, preferred_element_type=jnp.float32))
    selected = hidden
    channel_sum = summed_on_arrival(
        jnp.dot(selected, down_whole, preferred_element_type=jnp.float32).astype(jnp.bfloat16),
        "tp",
        0,
    )
    return (updated.astype(jnp.float32) + channel_sum).astype(jnp.bfloat16)


def solution(mesh):
    torus = Mesh(mesh.devices.reshape(4, 4, mesh.shape["tp"]), ("sp_0", "sp_1", "tp"))
    placed = (
        P(SP_TP, None),
        P(SP, "tp"),
        P(SP, "tp"),
        P(SP, "tp"),
        P(SP, "tp"),
        P("tp", SP),
        P("tp", None),
        P(),
        P(SP, "tp"),
        P("tp", SP),
    )
    return jax.shard_map(
        body, mesh=torus, in_specs=placed, out_specs=P(SP_TP, None), check_vma=False
    )
```

profile of v0, /device:TPU:1, one launch (start us, length us, event | category | flops | bytes accessed | tf_op | source)
XLA Modules:
  0.0 298.3 jit_solution(17015937021389001376)
XLA Ops:
  7.4 1.1 reduce_window_sum.20
  8.5 0.7 slice_reduce_fusion
  9.3 1.4 bitcast_convert_fusion
  10.7 3.1 %fusion.32 = (f32[1024,1,128]{2,0,1:T(8,128)S(1)}, f32[1024,1,128]{2,0,1:T(8,128)S(1)}, bf16[1024,1,128]{2,0,1:T(8,128)(2,1)S(1)}, bf16[1024,1,128]{2,0,1:T(8,128)(2,1)}) fusion(f32[1024,1,256]{2,0,1:T(8,128)S(1)} %get-tuple-element.114, f32[128]{0:T(128)S(1)} %multiply_power_fusion, f32[1024]{0:T(1024)S(1)} %add_convert_fusion.2, ...), kind=kLoop, calls=%fused_computation.54 | loop fusion | flops 1966080 | bytes 3674624 | tf_op jit(solution)/shard_map/sub | solution.py:81
  13.8 0.8 copy-done.4
  14.6 3.1 %convolution_bitcast_fusion = f32[8,1,256,512]{3,2,1,0:T(8,128)} fusion(bf16[8,128,512]{2,1,0:T(8,128)(2,1)S(1)} %bitcast.126, f32[8,128]{1,0:T(8,128)S(1)} %get-tuple-element.94, f32[8,128,128]{2,1,0:T(8,128)S(1)} %bitcast.121, f32[8,128,128]{2,1,0:T(8,128)S(1)} %bitcast.119), kind=kOutput, calls=%fused_computation.11 | convolution fusion | flops 270008320 | bytes 6295552 | tf_op jit(solution)/shard_map/njhd,njhv->nhdv/dot_general | solution.py:135
  17.7 27.6 %while.13 = (s32[]{:T(128)}, f32[1,256,512]{2,1,0:T(8,128)S(1)}, f32[8,1,256,512]{3,2,1,0:T(8,128)}, f32[8,1]{0,1:T(1,128)S(1)}, f32[8,1,256,512]{3,2,1,0:T(8,128)}, /*index=5*/s32[]{:T(128)}, s32[]{:T(128)}) while((s32[]{:T(128)}, f32[1,256,512]{2,1,0:T(8,128)S(1)}, f32[8,1,256,512]{3,2,1,0:T(8,128)}, f32[8,1]{0,1:T(1,128)S(1)}, ...), condition=%wide.region_4.5_spmd.clone, body=%wide.region_3.4_spmd.clone.sunk | while | flops 524291 | bytes 2622060 | solution.py:138
  17.7 0.9 bitcast_dynamic-update-slice_fusion.2
  18.5 0.7 constant_dynamic-slice_fusion.2
  19.2 1.9 bitcast_add_fusion.3
  21.1 0.8 bitcast_dynamic-update-slice_fusion.2
  22.0 0.7 constant_dynamic-slice_fusion.2
  22.6 1.9 bitcast_add_fusion.3
  24.6 0.9 bitcast_dynamic-update-slice_fusion.2
  25.4 0.7 constant_dynamic-slice_fusion.2
  26.1 1.9 bitcast_add_fusion.3
  28.0 0.8 bitcast_dynamic-update-slice_fusion.2
  28.9 0.7 constant_dynamic-slice_fusion.2
  29.5 1.9 bitcast_add_fusion.3
  31.5 0.8 bitcast_dynamic-update-slice_fusion.2
  32.3 0.7 constant_dynamic-slice_fusion.2
  33.0 1.9 bitcast_add_fusion.3
  34.9 0.8 bitcast_dynamic-update-slice_fusion.2
  35.7 0.7 constant_dynamic-slice_fusion.2
  36.4 1.9 bitcast_add_fusion.3
  38.3 0.8 bitcast_dynamic-update-slice_fusion.2
  39.2 0.7 constant_dynamic-slice_fusion.2
  39.8 1.9 bitcast_add_fusion.3
  41.8 0.9 bitcast_dynamic-update-slice_fusion.2
  42.7 0.7 constant_dynamic-slice_fusion.2
  43.3 1.9 bitcast_add_fusion.3
  45.2 0.7 convert_element_type.250
  47.2 0.7 dynamic-update-slice
  47.9 9.5 %all-reduce = bf16[4]{0:T(256)(128)(2,1)S(1)} all-reduce(bf16[4]{0:T(256)(128)(2,1)S(1)} %dynamic-update-slice), channel_id=1, replica_groups=mesh['sp_0'=4,'sp_1'=4,'tp'=8] {'sp_1'}, use_global_device_ids=true, to_apply=%add | all-reduce | flops 4 | bytes 16
  57.4 0.7 slice_convert_fusion.3
  58.8 12.6 %all-gather.12.cloned.1.call-done = bf16[4,256,512]{2,1,0:T(8,128)(2,1)} async-done(((bf16[1,256,512]{2,1,0:T(8,128)(2,1)}), bf16[4,256,512]{2,1,0:T(8,128)(2,1)}) %all-gather.12.cloned.1.call-update) | async-done | bytes 1048592 | tf_op jit(solution)/shard_map/all_gather | solution.py:29
  71.4 3.8 %fusion.36 = bf16[1,1,256,512]{3,2,1,0:T(8,128)(2,1)} fusion(f32[]{:T(128)} %bitcast.27, f32[]{:T(128)} %bitcast.28, f32[]{:T(128)} %bitcast.29, f32[]{:T(128)} %bitcast.30, bf16[4,256,512]{2,1,0:T(8,128)(2,1)} %all-gather.12.cloned.1.call-done), kind=kLoop, calls=%fused_computation.64 | loop fusion | flops 1572864 | bytes 1310736 | tf_op jit(solution)/shard_map/convert_element_type | solution.py:29
  75.3 0.6 dynamic-slice.1
  75.9 0.7 fusion.67
  76.6 1.3 dynamic-update-slice.1
  77.9 8.9 %all-reduce.1 = bf16[4]{0:T(256)(128)(2,1)S(1)} all-reduce(bf16[4]{0:T(256)(128)(2,1)S(1)} %dynamic-update-slice.1), channel_id=2, replica_groups=mesh['sp_0'=4,'sp_1'=4,'tp'=8] {'sp_0'}, use_global_device_ids=true, to_apply=%add.1 | all-reduce | flops 4 | bytes 16
  86.8 0.7 fusion.66
  92.7 3.4 %fusion.14 = f32[8,128,512]{2,1,0:T(8,128)} fusion(bf16[8,128,512]{2,1,0:T(8,128)(2,1)} %bitcast.125, bf16[8,128,128]{2,1,0:T(8,128)(2,1)S(1)} %bitcast.127, bf16[8,128,128]{2,1,0:T(8,128)(2,1)} %bitcast.129, f32[8,128]{1,0:T(8,128)S(1)} %bitcast.136, pred[128,128]{1,0:T(8,128)(4,1)S(1)} %iota_compare_fusion, f32[8,128,128]{2,1,0:T(8,128)} %bitcast.122, ...), kind=kOutput, calls=%fused_computation.30 | convolution fusion | flops 203816960 | bytes 4739072 | tf_op jit(solution)/shard_map/hnij,njhv->nihv/dot_general | solution.py:129
  96.1 4.0 %all-gather.8.cloned.1.call-done = bf16[4,1,256,512]{3,2,1,0:T(8,128)(2,1)} async-done(((bf16[1,1,256,512]{3,2,1,0:T(8,128)(2,1)}), bf16[4,1,256,512]{3,2,1,0:T(8,128)(2,1)}) %all-gather.8.cloned.1.call-update) | async-done | bytes 1048592 | tf_op jit(solution)/shard_map/all_gather | solution.py:29
  100.1 3.8 %fusion.35 = f32[256,512]{1,0:T(8,128)S(1)} fusion(bf16[4,1,256,512]{3,2,1,0:T(8,128)(2,1)} %all-gather.8.cloned.1.call-done, f32[]{:T(128)} %bitcast.27, f32[]{:T(128)} %bitcast.28, f32[]{:T(128)} %bitcast.29, f32[]{:T(128)} %bitcast.30, f32[]{:T(128)} %bitcast.26, f32[]{:T(128)S(6)} %convert.22, f32[]{:T(128)S(6)} %convert.21, f32[]{:T(128)S(6)} %convert.20, ...), kind=kLoop, calls=%fused_computation.61 | loop fusion | flops 4194304 | bytes 2621484 | tf_op jit(solution)/shard_map/mul | solution.py:150
  103.9 3.8 %fusion.7 = (f32[8,128]{1,0:T(8,128)S(1)}, f32[8,512,128]{1,2,0:T(8,128)S(1)}) fusion(f32[8,1,256,512]{3,2,1,0:T(8,128)} %get-tuple-element.34, f32[256,512]{1,0:T(8,128)S(1)} %fusion.35, f32[8]{0:T(128)S(1)} %fusion.50, f32[8,128]{1,0:T(8,128)S(1)} %get-tuple-element.93, bf16[8,128,128]{2,1,0:T(8,128)(2,1)S(1)} %bitcast.128, ...), kind=kOutput, calls=%fused_computation.20 | convolution fusion | flops 274725888 | bytes 9445408 | tf_op jit(solution)/shard_map/nihd,nhdv->nihv/dot_general | solution.py:153
  107.8 0.7 fusion.10
  108.5 4.3 %convolution_convert_fusion = bf16[1024,2048]{1,0:T(8,128)(2,1)} fusion(bf16[1024,512]{1,0:T(8,128)(2,1)S(1)} %bitcast.132, bf16[512,2048]{1,0:T(8,128)(2,1)S(1)} %copy-done), kind=kOutput, calls=%fused_computation.7 | convolution fusion | flops 2149580800 | bytes 7340032 | tf_op jit(solution)/shard_map/dot_general | solution.py:180
  112.9 0.9 copy-done.8
  113.8 0.8 pad_maximum_fusion.1
  114.9 35.9 %reduce-scatter.2.cloned.1.call-done = bf16[128,2048]{1,0:T(8,128)(2,1)} async-done(((bf16[1024,2048]{1,0:T(8,128)(2,1)}), bf16[128,2048]{1,0:T(8,128)(2,1)}) %reduce-scatter.2.cloned.1.call-update) | async-done | bytes 524304 | tf_op jit(solution)/shard_map/reduce_scatter | solution.py:179
  150.8 1.4 fusion.15
  152.2 2.1 fusion.17
  154.3 34.1 %all-gather.14.cloned.1.call-done = bf16[4194304]{0:T(1024)(128)(2,1)} async-done(((bf16[262144]{0:T(1024)(128)(2,1)}), bf16[4194304]{0:T(1024)(128)(2,1)}) %all-gather.14.cloned.1.call-update) | async-done | bytes 8388624 | tf_op jit(solution)/shard_map/all_gather | solution.py:52
  188.4 7.6 %reshape.504 = bf16[16,262144]{1,0:T(8,128)(2,1)} reshape(bf16[4194304]{0:T(1024)(128)(2,1)} %all-gather.14.cloned.1.call-done) | data formatting | bytes 16777216 | tf_op jit(solution)/shard_map/all_gather | solution.py:52
  196.1 5.6 %fusion.65 = (bf16[16,131072]{1,0:T(8,128)(2,1)}, bf16[2,8,1024,128]{3,1,2,0:T(8,128)(2,1)S(1)}) fusion(bf16[16,262144]{1,0:T(8,128)(2,1)} %reshape.504), kind=kLoop, calls=%fused_computation.106 | loop fusion | bytes 16777216 | tf_op jit(solution)/shard_map/slice | solution.py:54
  201.6 2.7 copy.25
  204.4 6.4 %copy.22 = bf16[1024,16,128]{0,2,1:T(8,128)(2,1)} copy(bf16[1024,16,128]{2,0,1:T(8,128)(2,1)} %bitcast.118) | data formatting | bytes 8388608 | tf_op jit(solution)/shard_map/transpose | solution.py:45
  210.8 4.8 %reshape_reshape.3 = bf16[2048,1024]{1,0:T(8,128)(2,1)} reshape(bf16[16,131072]{1,0:T(8,128)(2,1)} %get-tuple-element.85) | data formatting | bytes 8388608 | tf_op jit(solution)/shard_map/reshape;reshape | solution.py:47
  215.6 6.5 %all-gather.10.cloned.1.call-done = bf16[1024,2048]{1,0:T(8,128)(2,1)} async-done(((bf16[128,2048]{1,0:T(8,128)(2,1)}), bf16[1024,2048]{1,0:T(8,128)(2,1)}) %all-gather.10.cloned.1.call-update) | async-done | bytes 4194320 | tf_op jit(solution)/shard_map/all_gather | solution.py:188
  222.1 14.4 %convolution_convert_fusion.1 = bf16[1024,2048]{1,0:T(8,128)(2,1)} fusion(bf16[1024,2048]{0,1:T(8,128)(2,1)} %bitcast.123, bf16[1024,2048]{1,0:T(8,128)(2,1)} %all-gather.10.cloned.1.call-done, bf16[2048,1024]{1,0:T(8,128)(2,1)} %reshape_reshape.3), kind=kOutput, calls=%fused_computation.8 | convolution fusion | flops 8595177472 | bytes 16777216 | tf_op jit(solution)/shard_map/dot_general | solution.py:192
  236.5 52.6 %all_to_all.5 = bf16[8,128,2048]{2,1,0:T(8,128)(2,1)S(1)} all-to-all(bf16[8,128,2048]{2,1,0:T(8,128)(2,1)} %bitcast.124), channel_id=1, replica_groups=mesh['sp_0'=4,'sp_1'=4,'tp'=8] {'tp'}, dimensions={0} | all-to-all | bytes 8388608 | tf_op jit(solution)/shard_map/all_to_all | solution.py:68
  289.2 0.7 convert_reduce_fusion
  290.2 1.0 fusion.18
  (50 shorter events, 1.8 us)
Async XLA Ops:
  7.4 101.1 %copy-start = (bf16[512,2048]{1,0:T(8,128)(2,1)S(1)}, bf16[512,2048]{1,0:T(8,128)(2,1)}, u32[]{:S(2)}) copy-start(bf16[512,2048]{1,0:T(8,128)(2,1)} %param.18) | copy-start | bytes 6291460
  7.4 64.0 %all-gather.12.cloned.1.call-start = ((), (), s32[]{:S(2)}) async-start(), calls=%async_computation.5 | async-start | bytes 1310720 | tf_op jit(solution)/shard_map/all_gather | solution.py:29
  9.3 5.3 %copy-start.5 = (bf16[1024,512]{1,0:T(8,128)(2,1)S(1)}, bf16[1024,512]{1,0:T(8,128)(2,1)}, u32[]{:S(2)}) copy-start(bf16[1024,512]{1,0:T(8,128)(2,1)} %param.15) | copy-start | bytes 3145732
  13.8 0.8 copy-start.4
  17.7 29.0 %copy-start.12 = (u32[128]{0:T(128)S(1)}, u32[128]{0:T(128)}, u32[]{:S(2)}) copy-start(u32[128]{0:T(128)} %constant.76) | copy-start | bytes 1540
  17.7 57.6 %copy-start.11 = (u32[128]{0:T(128)S(1)}, u32[128]{0:T(128)}, u32[]{:S(2)}) copy-start(u32[128]{0:T(128)} %constant.81) | copy-start | bytes 1540
  46.0 54.1 %all-gather.8.cloned.1.call-start = ((), (), s32[]{:S(2)}) async-start(), calls=%async_computation.2 | async-start | bytes 1310720 | tf_op jit(solution)/shard_map/all_gather | solution.py:29
  75.2 28.7 %copy-start.6 = (bf16[1024,1,128]{2,0,1:T(8,128)(2,1)S(1)}, bf16[1024,1,128]{2,0,1:T(8,128)(2,1)}, u32[]{:S(2)}) copy-start(bf16[1024,1,128]{2,0,1:T(8,128)(2,1)} %get-tuple-element.92) | copy-start | bytes 786436
  75.3 75.5 %reduce-scatter.2.cloned.1.call-start = ((), (), s32[]{:S(2)}) async-start(), calls=%async_computation.3 | async-start | bytes 4718592 | tf_op jit(solution)/shard_map/reduce_scatter | solution.py:179
  103.9 3.8 %copy-start.7 = (bf16[1024,512]{1,0:T(8,128)(2,1)S(1)}, bf16[1024,512]{1,0:T(8,128)(2,1)}, u32[]{:S(2)}) copy-start(bf16[1024,512]{1,0:T(8,128)(2,1)} %param.16) | copy-start | bytes 3145732
  112.8 0.9 copy-start.8
  112.8 1.0 copy-start.9
  112.8 2.1 copy-start.10
  112.8 38.0 %copy-start.2 = (bf16[128,2048]{1,0:T(8,128)(2,1)S(1)}, bf16[128,2048]{1,0:T(8,128)(2,1)}, u32[]{:S(2)}) copy-start(bf16[128,2048]{1,0:T(8,128)(2,1)} %param.12) | copy-start | bytes 1572868
  112.8 75.6 %all-gather.14.cloned.1.call-start = ((), (), s32[]{:S(2)}) async-start(), calls=%async_computation.6 | async-start | bytes 8912896 | tf_op jit(solution)/shard_map/all_gather | solution.py:52
  114.7 107.5 %all-gather.10.cloned.1.call-start = ((), (), s32[]{:S(2)}) async-start(), calls=%async_computation.4 | async-start | bytes 4718592 | tf_op jit(solution)/shard_map/all_gather | solution.py:188
  236.5 54.7 %copy-start.1 = (bf16[512,2048]{1,0:T(8,128)(2,1)S(1)}, bf16[512,2048]{1,0:T(8,128)(2,1)}, u32[]{:S(2)}) copy-start(bf16[512,2048]{1,0:T(8,128)(2,1)} %param.18) | copy-start | bytes 6291460
  289.2 1.0 copy-start.3
Sparse Core Ops, SparseCore 0:
  46.1 25.2 all-gather.11
  75.4 24.6 all-gather.7
  112.9 37.7 reduce-scatter.1
Sparse Core Ops, SparseCore 1:
  115.4 72.9 all-gather.13
  190.0 32.1 all-gather.9
where the time goes:
time: 300 us; the launch traced here: 298 us
  waiting for transfers between devices  93.2 us (31%)
  blocking collectives  71.1 us (24%)
  other arithmetic  45.1 us (15%)
  local copies, waits for them, and re-layouts  38.4 us (13%)
  matrix products  29 us (10%)
  between operations  21.1 us (7%)
    all_to_all x1, blocking collectives, summed_on_arrival(): lax.all_to_all(tiles, axis, split_axis=0, concat_axis=0, tiled=True)  52.6 us
    reduce_scatter x1, waiting for transfers between devices, body(): lax.psum_scatter(jnp.dot(selected, retention_output_weight, preferred_ele...  35.9 us
    all_gather x1, waiting for transfers between devices, gather_packed(): lines, at, gathered = (lax.all_gather(flat, axis), 0, [])  34.1 us
    unnamed x2, blocking collectives  18.5 us
    all_gather x2, waiting for transfers between devices, carried_in(): lax.all_gather(part.astype(kind), axis)  16.6 us
    add x8, other arithmetic, carry_step(): return (decay[:, None, None] * prior + term, prior)  15.3 us
    dot_general x1, matrix products, body(): jnp.dot(selected, down_whole, preferred_element_type=jnp.float32)  14.4 us
    unnamed x34, local copies, waits for them, and re-layouts  7.93 us
  transfers between devices with their start and end apart: 5, of which 5 were waited for; matrix products, arithmetic and copies ran while one was open for 13% of the time, Pallas kernels for 0%

commit v1 on v0

v1 whole, which is shorter than its diff:
```python
import jax
import jax.numpy as jnp
import numpy as np
from jax import lax
from jax.experimental import pallas as pl
from jax.experimental.pallas import tpu as pltpu
from jax.sharding import Mesh
from jax.sharding import PartitionSpec as P

DK = 256
DV = 512
HALF = DK // 2
BLOCK = 128
BLOCKS = 8
ROWS = 1024
D = 2048
FFL = 1024
QUARTER = DK // 4
EPS = 1e-06
F32 = jnp.float32
BF16 = jnp.bfloat16


def rotation_tables():
    inverse = 10000.0 ** (-np.arange(0, DK, 2, dtype=np.float64) / DK)
    inside = np.arange(BLOCK, dtype=np.float64)[:, None] * inverse[None, :]
    start = (np.arange(128, dtype=np.float64) * BLOCK)[:, None] * inverse[None, :]
    return np.stack([np.cos(inside), np.sin(inside), np.cos(start), np.sin(start)]).astype(np.float32)


class Copies:
    def __init__(self, send, recv):
        self.send, self.recv, self.count, self.made = send, recv, 0, []

    def start(self, src, dst, **where):
        copy = pltpu.make_async_remote_copy(
            src_ref=src,
            dst_ref=dst,
            send_sem=self.send.at[self.count],
            recv_sem=self.recv.at[self.count],
            device_id=where,
            device_id_type=pl.DeviceIdType.MESH,
        )
        copy.start()
        self.count += 1
        self.made.append(copy)
        return copy

    def finish(self):
        for copy in self.made:
            copy.wait_send()


N_COPIES = 64
N_LOCAL = 16


def kernel(
    resid, q_in, k_in, v_in, g_in, ld_in, wo_in, gain_in, up_in, dn_in, tab_in, out,
    q_s, k_s, v_s, g_s, wo_s, resid_s, gain_s, ld_s, tab_s,
    ccol, crow, bstart, s_run, s_blk, local, q_late, gated,
    st_tx, st_rx, in_tx, in_rx, row_tx, row_rx, dec_tx, dec_rx, rdec_tx, rdec_rx,
    p1, p1_rx, ra1_p, ra1_m, rb1_p, rb1_m,
    updated, normed, hidden, up_w, dn_w,
    p2, p2_rx, ra2_p, ra2_m, rb2_p, rb2_m,
    send, recv, loc,
):
    z, y = lax.axis_index("z"), lax.axis_index("y")
    x, c = lax.axis_index("x"), lax.axis_index("c")

    def step(a, by):
        return lax.rem(a + by, 4)

    xp, xm, xo = step(x, 1), step(x, 3), step(x, 2)
    yp, ym = step(y, 1), step(y, 3)
    zp, zm = step(z, 1), step(z, 3)
    other = 1 - c
    net = Copies(send, recv)

    local_copies = []

    def fetch(src, dst):
        copy = pltpu.make_async_copy(src, dst, loc.at[len(local_copies)])
        copy.start()
        local_copies.append(copy)
        return copy

    own_rows = pl.ds(pl.multiple_of((4 * z + y) * 128, 128), 128)
    own_cols = pl.ds(pl.multiple_of((4 * y + z) * 128, 128), 128)

    barrier = pltpu.get_barrier_semaphore()
    for where in (
        {"y": yp}, {"y": ym}, {"y": step(y, 2)},
        {"z": zp}, {"z": zm}, {"z": step(z, 2)},
        {"x": xp}, {"x": xm}, {"c": other},
    ):
        pl.semaphore_signal(barrier, inc=1, device_id=where, device_id_type=pl.DeviceIdType.MESH)

    f_ld = fetch(ld_in, ld_s)
    f_tab = fetch(tab_in, tab_s)
    f_k = fetch(k_in, k_s)
    f_v = fetch(v_in, v_s)
    f_q = fetch(q_in, q_s)
    f_g = fetch(g_in, g_s)
    f_wo = fetch(wo_in, wo_s)
    f_res = fetch(resid, resid_s)
    f_gain = fetch(gain_in, gain_s)
    f_up = fetch(up_in, up_w.at[own_rows, :])
    f_dn = fetch(dn_in, dn_w.at[:, own_cols])

    pl.semaphore_wait(barrier, 9)

    u1p = net.start(up_in, up_w.at[own_rows, :], y=yp)
    u1m = net.start(up_in, up_w.at[own_rows, :], y=ym)
    d1p = net.start(dn_in, dn_w.at[:, own_cols], z=zp)
    d1m = net.start(dn_in, dn_w.at[:, own_cols], z=zm)

    f_ld.wait()
    ii = lax.broadcasted_iota(jnp.int32, (BLOCK, BLOCK), 0)
    jj = lax.broadcasted_iota(jnp.int32, (BLOCK, BLOCK), 1)
    causal = ii >= jj
    lower = jnp.where(causal, 1.0, 0.0).astype(F32)
    ld = ld_s[...]
    nt = (((1,), (1,)), ((), ()))
    by_col = lax.dot_general(lower, ld, nt, precision=lax.Precision.HIGHEST, preferred_element_type=F32)
    crow[...] = lax.dot_general(ld, lower, nt, precision=lax.Precision.HIGHEST, preferred_element_type=F32)
    for n in range(BLOCKS):
        ccol[n * BLOCK : (n + 1) * BLOCK, :] = jnp.broadcast_to(by_col[:, n : n + 1], (BLOCK, 128))

    f_tab.wait()
    f_k.wait()
    f_v.wait()

    def rotated(ref, n):
        rows = pl.ds(pl.multiple_of(n * BLOCK, BLOCK), BLOCK)
        block = (4 * z + y) * BLOCKS + n
        cos_in, sin_in = tab_s[0], tab_s[1]
        cos_at = tab_s[2, pl.ds(block, 1), :]
        sin_at = tab_s[3, pl.ds(block, 1), :]
        cosine = cos_at * cos_in - sin_at * sin_in
        sine = sin_at * cos_in + cos_at * sin_in
        first = ref[rows, 0:HALF].astype(F32)
        second = ref[rows, HALF:DK].astype(F32)
        return rows, first * cosine - second * sine, first * sine + second * cosine

    s_run[...] = jnp.zeros_like(s_run)

    def state_block(n, before):
        rows, a, b = rotated(k_s, n)
        a = (a * DK**-0.5).astype(BF16)
        b = (b * DK**-0.5).astype(BF16)
        k_s[rows, 0:HALF] = a
        k_s[rows, HALF:DK] = b
        total = ccol[pl.ds(n * BLOCK + BLOCK - 1, 1), :]
        to_end = jnp.exp(total - ccol[rows, :])
        decayed = jnp.concatenate(
            [(a.astype(F32) * to_end).astype(BF16), (b.astype(F32) * to_end).astype(BF16)], axis=1
        )
        term = lax.dot_general(
            decayed, v_s[rows, :], (((0,), (0,)), ((), ())), preferred_element_type=F32
        )
        s_blk[n] = s_run[...].astype(BF16)
        s_run[...] = jnp.exp(total[:, 0:1]) * s_run[...] + term
        bstart[pl.ds(n, 1), :] = before
        return before + total

    total = lax.fori_loop(0, BLOCKS, state_block, jnp.zeros((1, 128), F32))

    dec_tx[...] = jnp.broadcast_to(total, (8, 128))
    dec_rx[y] = jnp.broadcast_to(total, (8, 128))
    for part in range(4):
        st_tx[part] = s_run[part * QUARTER : (part + 1) * QUARTER, :].astype(BF16)
    st_copies = []
    for by in (1, 3, 2):
        to = step(y, by)
        st_copies.append(net.start(dec_tx, dec_rx.at[y], y=to))
        st_copies.append(net.start(st_tx.at[to], st_rx.at[y], y=to))
    st_rx[y] = st_tx[y]

    def up_rows(zz, yy, first, size):
        return pl.ds(pl.multiple_of(zz * 512 + yy * 128 + first, 64), size)

    def dn_cols(yy, zz):
        return pl.ds(pl.multiple_of(yy * 512 + zz * 128, 128), 128)

    u1p.wait_recv()
    here = up_w.at[up_rows(z, ym, 0, 64), :]
    u1fp = net.start(here, here, y=yp)
    u1m.wait_recv()
    here = up_w.at[up_rows(z, yp, 64, 64), :]
    u1fm = net.start(here, here, y=ym)
    d1p.wait_recv()
    here = dn_w.at[0:512, dn_cols(y, zm)]
    d1fp = net.start(here, here, z=zp)
    d1m.wait_recv()
    here = dn_w.at[512:1024, dn_cols(y, zp)]
    d1fm = net.start(here, here, z=zm)

    f_q.wait()
    f_g.wait()

    def local_block(n, carry):
        rows, a, b = rotated(q_s, n)
        col = ccol[rows, :]
        a = a.astype(BF16)
        b = b.astype(BF16)
        query = jnp.concatenate([a, b], axis=1)
        scores = lax.dot_general(query, k_s[rows, :], nt, preferred_element_type=F32)
        spread = col - crow[pl.ds(n, 1), :]
        factor = jnp.where(causal, jnp.exp(jnp.minimum(spread, 0.0)), 0.0)
        weights = (scores * factor).astype(BF16)
        a = a.astype(F32)
        b = b.astype(F32)
        early = jnp.exp(col)
        decayed = jnp.concatenate([(a * early).astype(BF16), (b * early).astype(BF16)], axis=1)
        late = jnp.exp(col + bstart[pl.ds(n, 1), :])
        q_late[rows, 0:HALF] = (a * late).astype(BF16)
        q_late[rows, HALF:DK] = (b * late).astype(BF16)
        local[rows, :] = jnp.dot(
            weights, v_s[rows, :], preferred_element_type=F32
        ) + jnp.dot(decayed, s_blk[n], preferred_element_type=F32)
        return carry

    lax.fori_loop(0, 4, local_block, 0)

    for copy in st_copies:
        copy.wait_recv()
    run = st_rx[0].astype(F32)
    log_row = dec_rx[0]
    for at in range(1, 4):
        run = jnp.exp(dec_rx[at][0:1, 0:1]) * run + st_rx[at].astype(F32)
        log_row = log_row + dec_rx[at]
    row_tx[...] = run.astype(BF16)
    row_rx[z] = run.astype(BF16)
    rdec_tx[...] = log_row
    rdec_rx[z] = log_row
    row_copies = []
    for by in (1, 3, 2):
        to = step(z, by)
        row_copies.append(net.start(rdec_tx, rdec_rx.at[z], z=to))
        row_copies.append(net.start(row_tx, row_rx.at[z], z=to))

    lax.fori_loop(4, 8, local_block, 0)

    for copy in row_copies:
        copy.wait_recv()
    run = jnp.zeros((QUARTER, DV), F32)
    for at in range(4):
        later = jnp.exp(rdec_rx[at][0:1, 0:1]) * run + row_rx[at].astype(F32)
        run = jnp.where(at < z, later, run)
    for at in range(4):
        in_tx[at] = run.astype(BF16)
        if at < 3:
            run = jnp.exp(dec_rx[at][0:1, 0:1]) * run + st_rx[at].astype(F32)
    in_copies = []
    for by in (1, 3, 2):
        to = step(y, by)
        in_copies.append(net.start(in_tx.at[to], in_rx.at[y], y=to))
    in_rx[y] = in_tx[y]

    u1fp.wait_recv()
    u1fm.wait_recv()
    d1fp.wait_recv()
    d1fm.wait_recv()
    f_up.wait()
    f_dn.wait()

    def up_half(zz, half):
        return up_w.at[pl.ds(pl.multiple_of(zz * 512 + half * 256, 256), 256), :]

    def dn_half(yy, half):
        return dn_w.at[half * 512 : (half + 1) * 512, pl.ds(pl.multiple_of(yy * 512, 512), 512)]

    u2p = net.start(up_half(z, 0), up_half(z, 0), z=zp)
    u2m = net.start(up_half(z, 1), up_half(z, 1), z=zm)
    d2p = net.start(dn_half(y, 0), dn_half(y, 0), y=yp)
    d2m = net.start(dn_half(y, 1), dn_half(y, 1), y=ym)
    u3p = net.start(up_half(z, 1), up_half(z, 1), z=zp)
    u3m = net.start(up_half(z, 0), up_half(z, 0), z=zm)
    d3p = net.start(dn_half(y, 1), dn_half(y, 1), y=yp)
    d3m = net.start(dn_half(y, 0), dn_half(y, 0), y=ym)

    f_wo.wait()
    f_res.wait()
    f_gain.wait()
    for copy in in_copies:
        copy.wait_recv()

    def gate_rows(d):
        def part(i, carry):
            rows = pl.ds(pl.multiple_of(d * 256 + i * 128, 128), 128)
            incoming = jnp.concatenate([in_rx[at] for at in range(4)], axis=0)
            kept = local[rows, :] + jnp.dot(q_late[rows, :], incoming, preferred_element_type=F32)
            scale = lax.rsqrt(jnp.mean(kept * kept, axis=-1, keepdims=True) + EPS)
            gate = g_s[rows, :].astype(F32)
            gate = gate / (1.0 + jnp.exp(-gate))
            gated[pl.ds(pl.multiple_of(i * 128, 128), 128), :] = (gate * kept * scale).astype(BF16)
            return carry

        lax.fori_loop(0, 2, part, 0)

    def project(d):
        gate_rows(d)
        for j in range(4):
            part = jnp.dot(
                gated[...], wo_s[:, j * 512 : (j + 1) * 512], preferred_element_type=F32
            ).astype(BF16)
            to = slice((j % 2) * 512, (j % 2) * 512 + 512)
            p1[d, 0, j // 2, :, to] = part[0:128]
            p1[d, 1, j // 2, :, to] = part[128:256]

    def accumulate(p, d, half, extra):
        p[d, c, half] = (p[d, c, half].astype(F32) + extra[...].astype(F32)).astype(BF16)

    def pair(p, p_rx, d):
        return net.start(p.at[d, other], p_rx.at[d], c=other)

    def pair_sum(copy, p, p_rx, d):
        copy.wait_recv()
        for half in range(2):
            accumulate(p, d, half, p_rx.at[d, half])

    project(xo)
    w_o = pair(p1, p1_rx, xo)
    project(xp)
    w_p = pair(p1, p1_rx, xp)
    pair_sum(w_o, p1, p1_rx, xo)
    a_p = net.start(p1.at[xo, c, 0], ra1_p, x=xp)
    a_m = net.start(p1.at[xo, c, 1], ra1_m, x=xm)
    project(xm)
    w_m = pair(p1, p1_rx, xm)
    pair_sum(w_p, p1, p1_rx, xp)
    b_p = net.start(p1.at[xp, c, 1], rb1_p.at[1], x=xp)
    project(x)
    w_s = pair(p1, p1_rx, x)
    pair_sum(w_m, p1, p1_rx, xm)
    b_m = net.start(p1.at[xm, c, 0], rb1_m.at[0], x=xm)
    a_p.wait_recv()
    accumulate(p1, xp, 0, ra1_p)
    c_p = net.start(p1.at[xp, c, 0], rb1_p.at[0], x=xp)
    a_m.wait_recv()
    accumulate(p1, xm, 1, ra1_m)
    c_m = net.start(p1.at[xm, c, 1], rb1_m.at[1], x=xm)
    w_s.wait_recv()

    u2p.wait_recv()
    u2fp = net.start(up_half(zm, 0), up_half(zm, 0), z=zp)
    u2m.wait_recv()
    u2fm = net.start(up_half(zp, 1), up_half(zp, 1), z=zm)
    d2p.wait_recv()
    d2fp = net.start(dn_half(ym, 0), dn_half(ym, 0), y=yp)
    d2m.wait_recv()
    d2fm = net.start(dn_half(yp, 1), dn_half(yp, 1), y=ym)

    for copy in (b_p, b_m, c_p, c_m):
        copy.wait_recv()

    def norm_rows(i, carry):
        rows = pl.ds(pl.multiple_of(i * 32, 32), 32)
        halves = []
        for half in range(2):
            cols = slice(half * 1024, (half + 1) * 1024)
            value = p1[x, c, half, rows, :].astype(F32) + p1_rx[x, half, rows, :].astype(F32)
            value = value + (rb1_p[half, rows, :].astype(F32) + rb1_m[half, rows, :].astype(F32))
            value = (resid_s[rows, cols].astype(F32) + value).astype(BF16)
            updated[rows, cols] = value
            halves.append(value.astype(F32))
        square = sum(jnp.sum(v * v, axis=-1, keepdims=True) for v in halves)
        scale = lax.rsqrt(square * (1.0 / D) + EPS)
        for half in range(2):
            cols = slice(half * 1024, (half + 1) * 1024)
            normed[x, c, rows, cols] = (halves[half] * scale * gain_s[:, cols]).astype(BF16)
        return carry

    lax.fori_loop(0, 4, norm_rows, 0)

    own = normed.at[x, c]
    n_c = net.start(own, own, c=other)
    n_p = net.start(own, own, x=xp)
    n_m = net.start(own, own, x=xm)

    for copy in (u3p, u3m, d3p, d3m, u2fp, u2fm, d2fp, d2fm):
        copy.wait_recv()

    def mix(d):
        rows = normed[d].reshape(256, D)
        for j in range(2):
            cols = slice(j * 512, (j + 1) * 512)
            pre = jnp.maximum(jnp.dot(rows, up_w[:, cols], preferred_element_type=F32), 0.0)
            hidden[:, cols] = (pre * pre).astype(BF16)
        for yy in range(4):
            part = jnp.dot(
                hidden[...], dn_w[:, yy * 512 : (yy + 1) * 512], preferred_element_type=F32
            ).astype(BF16)
            for zz in range(4):
                to = slice(((zz % 2) * 4 + yy) * 128, ((zz % 2) * 4 + yy) * 128 + 128)
                piece = part[:, zz * 128 : (zz + 1) * 128]
                p2[d, 0, zz // 2, :, to] = piece[0:128]
                p2[d, 1, zz // 2, :, to] = piece[128:256]

    n_c.wait_recv()
    mix(x)
    w_s = pair(p2, p2_rx, x)
    n_p.wait_recv()
    came = normed.at[xm, c]
    half_row = normed.at[xm, c, 0:64, :]
    n_fp = net.start(half_row, half_row, x=xp)
    n_cm = net.start(came, came, c=other)
    n_m.wait_recv()
    came = normed.at[xp, c]
    half_row = normed.at[xp, c, 64:128, :]
    n_fm = net.start(half_row, half_row, x=xm)
    n_cp = net.start(came, came, c=other)
    n_cp.wait_recv()
    mix(xp)
    w_p = pair(p2, p2_rx, xp)
    n_fp.wait_recv()
    here = normed.at[xo, c, 0:64, :]
    n_c0 = net.start(here, here, c=other)
    n_fm.wait_recv()
    here = normed.at[xo, c, 64:128, :]
    n_c1 = net.start(here, here, c=other)
    pair_sum(w_p, p2, p2_rx, xp)
    b_p = net.start(p2.at[xp, c, 1], rb2_p.at[1], x=xp)
    n_cm.wait_recv()
    mix(xm)
    w_m = pair(p2, p2_rx, xm)
    n_c0.wait_recv()
    n_c1.wait_recv()
    pair_sum(w_m, p2, p2_rx, xm)
    b_m = net.start(p2.at[xm, c, 0], rb2_m.at[0], x=xm)
    mix(xo)
    w_o = pair(p2, p2_rx, xo)
    pair_sum(w_o, p2, p2_rx, xo)
    a_p = net.start(p2.at[xo, c, 0], ra2_p, x=xp)
    a_m = net.start(p2.at[xo, c, 1], ra2_m, x=xm)
    w_s.wait_recv()
    a_p.wait_recv()
    accumulate(p2, xp, 0, ra2_p)
    c_p = net.start(p2.at[xp, c, 0], rb2_p.at[0], x=xp)
    a_m.wait_recv()
    accumulate(p2, xm, 1, ra2_m)
    c_m = net.start(p2.at[xm, c, 1], rb2_m.at[1], x=xm)
    for copy in (b_p, b_m, c_p, c_m):
        copy.wait_recv()

    def final_rows(i, carry):
        rows = pl.ds(pl.multiple_of(i * 32, 32), 32)
        for half in range(2):
            cols = slice(half * 1024, (half + 1) * 1024)
            value = p2[x, c, half, rows, :].astype(F32) + p2_rx[x, half, rows, :].astype(F32)
            value = value + (rb2_p[half, rows, :].astype(F32) + rb2_m[half, rows, :].astype(F32))
            out[rows, cols] = (updated[rows, cols].astype(F32) + value).astype(BF16)
        return carry

    lax.fori_loop(0, 4, final_rows, 0)
    net.finish()


def body(resid, q, k, v, g, log_decay, wo, gain, up, dn):
    vm = pltpu.VMEM
    scratch = [
        vm((ROWS, DK), BF16), vm((ROWS, DK), BF16), vm((ROWS, DV), BF16), vm((ROWS, DV), BF16),
        vm((DV, D), BF16), vm((128, D), BF16), vm((1, D), F32), vm((BLOCKS, 128), F32),
        vm((4, 128, 128), F32),
        vm((ROWS, 128), F32), vm((BLOCKS, 128), F32), vm((BLOCKS, 128), F32),
        vm((DK, DV), F32), vm((BLOCKS, DK, DV), BF16), vm((ROWS, DV), F32), vm((ROWS, DK), BF16),
        vm((256, DV), BF16),
        vm((4, QUARTER, DV), BF16), vm((4, QUARTER, DV), BF16),
        vm((4, QUARTER, DV), BF16), vm((4, QUARTER, DV), BF16),
        vm((QUARTER, DV), BF16), vm((4, QUARTER, DV), BF16),
        vm((8, 128), F32), vm((4, 8, 128), F32), vm((8, 128), F32), vm((4, 8, 128), F32),
        vm((4, 2, 2, 128, 1024), BF16), vm((4, 2, 128, 1024), BF16),
        vm((128, 1024), BF16), vm((128, 1024), BF16),
        vm((2, 128, 1024), BF16), vm((2, 128, 1024), BF16),
        vm((128, D), BF16), vm((4, 2, 128, D), BF16), vm((256, FFL), BF16),
        vm((D, FFL), BF16), vm((FFL, D), BF16),
        vm((4, 2, 2, 128, 1024), BF16), vm((4, 2, 128, 1024), BF16),
        vm((128, 1024), BF16), vm((128, 1024), BF16),
        vm((2, 128, 1024), BF16), vm((2, 128, 1024), BF16),
        pltpu.SemaphoreType.DMA((N_COPIES,)),
        pltpu.SemaphoreType.DMA((N_COPIES,)),
        pltpu.SemaphoreType.DMA((N_LOCAL,)),
    ]
    anywhere = pl.BlockSpec(memory_space=pl.ANY)
    return pl.pallas_call(
        kernel,
        out_shape=jax.ShapeDtypeStruct((128, D), BF16),
        in_specs=[anywhere] * 11,
        out_specs=pl.BlockSpec(memory_space=pltpu.VMEM),
        scratch_shapes=scratch,
        compiler_params=pltpu.CompilerParams(
            collective_id=0, has_side_effects=True, vmem_limit_bytes=66_000_000
        ),
    )(
        resid, q, k, v, g, log_decay.reshape(BLOCKS, BLOCK), wo,
        gain.astype(F32).reshape(1, D), up, dn, jnp.asarray(rotation_tables()),
    )


def solution(mesh):
    torus = Mesh(mesh.devices.reshape(4, 4, 4, 2), ("z", "y", "x", "c"))
    sp, tp = ("z", "y"), ("x", "c")
    placed = (
        P(("z", "y", "x", "c"), None),
        P(sp, tp),
        P(sp, tp),
        P(sp, tp),
        P(sp, tp),
        P(tp, sp),
        P(tp, None),
        P(),
        P(sp, tp),
        P(tp, sp),
    )
    return jax.shard_map(
        body, mesh=torus, in_specs=placed, out_specs=P(("z", "y", "x", "c"), None), check_vma=False
    )
```

time: 300 us -> 105 us (0.35)
  Pallas kernels: 0 us -> 102 us
  waiting for transfers between devices: 93.2 us -> 0 us
  blocking collectives: 71.1 us -> 0 us
  other arithmetic: 45.1 us -> 1.29 us
  local copies, waits for them, and re-layouts: 38.4 us -> 1.88 us
  matrix products: 29 us -> 0 us
  between operations: 21.1 us -> 0.01 us
    pallas_call x0 -> x1, Pallas kernels: none -> 102 us  [body(): pl.pallas_call(kernel, out_shape=jax.ShapeDtypeStruct((128, D), BF16), in...]
    all_gather x4 -> x0, waiting for transfers between devices: 57.2 us -> none  [the longest x1 34.1 us: gather_packed(): lines, at, gathered = (lax.all_gather(flat, axis), 0, [])]
    all_to_all x1 -> x0, blocking collectives: 52.6 us -> none  [summed_on_arrival(): lax.all_to_all(tiles, axis, split_axis=0, concat_axis=0, tiled=True)]
    reduce_scatter x1 -> x0, waiting for transfers between devices: 35.9 us -> none  [body(): lax.psum_scatter(jnp.dot(selected, retention_output_weight, preferred_ele...]
    dot_general x5 -> x0, matrix products: 29 us -> none  [the longest x1 14.4 us: body(): jnp.dot(selected, down_whole, preferred_element_type=jnp.float32)]
    unnamed x2 -> x0, blocking collectives: 18.5 us -> none
    add x8 -> x0, other arithmetic: 15.3 us -> none  [carry_step(): return (decay[:, None, None] * prior + term, prior)]
    convert_element_type x10 -> x0, other arithmetic: 11.1 us -> none  [the longest x3 5.22 us: carried_in(): part.astype(kind)]
  transfers between devices with their start and end apart: 5 -> 0, of which waited for: 5 -> 0; matrix products, arithmetic and copies ran while one was open for 13% -> 0% of each run, Pallas kernels for 0% -> 0%
where the time goes in v1:
time: 105 us
  Pallas kernels  102 us (97%)
  local copies, waits for them, and re-layouts  1.88 us (2%)
  other arithmetic  1.29 us (1%)
    pallas_call x1, Pallas kernels, body(): pl.pallas_call(kernel, out_shape=jax.ShapeDtypeStruct((128, D), BF16), in...  102 us

profile of v1, /device:TPU:1, one launch (start us, length us, event | category | flops | bytes accessed | tf_op | source)
XLA Modules:
  0.0 105.1 jit_solution(102023178442213885)
XLA Ops:
  0.0 1.3 %reshape.11 = f32[2048]{0:T(1024)} convert(bf16[2048]{0:T(1024)(128)(2,1)} %param.18) | non-fusion elementwise | flops 2048 | bytes 12288 | tf_op jit(solution)/shard_map/reshape | solution.py:497
  1.3 101.9 %shard_map.109 = bf16[128,2048]{1,0:T(8,128)(2,1)} custom-call(bf16[128,2048]{1,0:T(8,128)(2,1)} %resid.1, bf16[1024,256]{1,0:T(8,128)(2,1)} %q_in.1, bf16[1024,256]{1,0:T(8,128)(2,1)} %k_in.1, bf16[1024,512]{1,0:T(8,128)(2,1)} %v_in.1, bf16[1024,512]{1,0:T(8,128)(2,1)} %g_in.1, f32[8,128]{1,0:T(8,128)} %bitcast.3, bf16[512,2048]{1,0:T(8,128)(2,1)} %wo_in.1, ...), custom_call_target="tpu_custom_call" | custom-call | tf_op jit(solution)/shard_map/pallas_call | solution.py:486
  103.2 1.9 %copy.13 = bf16[128,2048]{1,0:T(8,128)(2,1)} copy(bf16[128,2048]{1,0:T(8,128)(2,1)} %shard_map.109) | data formatting | bytes 1048576

commit v2 on v1

v2 whole, which is shorter than its diff:
```python
import jax
import jax.numpy as jnp
import numpy as np
from jax import lax
from jax.experimental import pallas as pl
from jax.experimental.pallas import tpu as pltpu
from jax.sharding import Mesh
from jax.sharding import PartitionSpec as P

DK = 256
DV = 512
HALF = DK // 2
BLOCK = 128
BLOCKS = 8
ROWS = 1024
D = 2048
FFL = 1024
QUARTER = DK // 4
EPS = 1e-06
F32 = jnp.float32
BF16 = jnp.bfloat16


def rotation_tables():
    inverse = 10000.0 ** (-np.arange(0, DK, 2, dtype=np.float64) / DK)
    inside = np.arange(BLOCK, dtype=np.float64)[:, None] * inverse[None, :]
    start = (np.arange(128, dtype=np.float64) * BLOCK)[:, None] * inverse[None, :]
    return np.stack([np.cos(inside), np.sin(inside), np.cos(start), np.sin(start)]).astype(np.float32)


class Phases:
    def __init__(self):
        self.scope = None

    def __call__(self, name):
        if self.scope is not None:
            self.scope.__exit__(None, None, None)
        self.scope = None
        if name is not None:
            self.scope = jax.named_scope(name)
            self.scope.__enter__()


class Copies:
    def __init__(self, send, recv):
        self.send, self.recv, self.count, self.made = send, recv, 0, []

    def start(self, src, dst, **where):
        copy = pltpu.make_async_remote_copy(
            src_ref=src,
            dst_ref=dst,
            send_sem=self.send.at[self.count],
            recv_sem=self.recv.at[self.count],
            device_id=where,
            device_id_type=pl.DeviceIdType.MESH,
        )
        copy.start()
        self.count += 1
        self.made.append(copy)
        return copy

    def finish(self):
        for copy in self.made:
            copy.wait_send()


N_COPIES = 128
N_LOCAL = 16


def kernel(
    resid, q_in, k_in, v_in, g_in, ld_in, wo_in, gain_in, up_in, dn_in, tab_in, out,
    q_s, k_s, v_s, g_s, wo_s, resid_s, gain_s, ld_s, tab_s,
    ccol, crow, bstart, s_run, s_blk, local, q_late, gated, gate_f,
    st_tx, st_rx, in_tx, in_rx, row_tx, row_rx, dec_tx, dec_rx, rdec_tx, rdec_rx,
    p1, p1_rx, ra1_p, ra1_m, rb1_p, rb1_m,
    updated, normed, hidden, up_w, dn_w,
    p2, p2_rx, ra2_p, ra2_m, rb2_p, rb2_m, out_s,
    send, recv, loc,
):
    z, y = lax.axis_index("z"), lax.axis_index("y")
    x, c = lax.axis_index("x"), lax.axis_index("c")

    def step(a, by):
        return lax.rem(a + by, 4)

    xp, xm, xo = step(x, 1), step(x, 3), step(x, 2)
    yp, ym = step(y, 1), step(y, 3)
    zp, zm = step(z, 1), step(z, 3)
    other = 1 - c
    net = Copies(send, recv)
    phase = Phases()
    phase("s00_barrier")

    local_copies = []

    def fetch(src, dst):
        copy = pltpu.make_async_copy(src, dst, loc.at[len(local_copies)])
        copy.start()
        local_copies.append(copy)
        return copy

    own_rows = pl.ds(pl.multiple_of((4 * z + y) * 128, 128), 128)
    own_cols = pl.ds(pl.multiple_of((4 * y + z) * 128, 128), 128)

    barrier = pltpu.get_barrier_semaphore()
    for where in (
        {"y": yp}, {"y": ym}, {"y": step(y, 2)},
        {"z": zp}, {"z": zm}, {"z": step(z, 2)},
        {"x": xp}, {"x": xm}, {"c": other},
    ):
        pl.semaphore_signal(barrier, inc=1, device_id=where, device_id_type=pl.DeviceIdType.MESH)

    f_ld = fetch(ld_in, ld_s)
    f_tab = fetch(tab_in, tab_s)
    f_k = fetch(k_in, k_s)
    f_v = fetch(v_in, v_s)
    f_q = fetch(q_in, q_s)
    f_g = fetch(g_in, g_s)
    f_wo = fetch(wo_in, wo_s)
    f_res = fetch(resid, resid_s)
    f_gain = fetch(gain_in, gain_s)
    f_up = fetch(up_in, up_w.at[own_rows, :])
    f_dn = fetch(dn_in, dn_w.at[:, own_cols])

    phase("s01_decays")
    f_ld.wait()
    ii = lax.broadcasted_iota(jnp.int32, (BLOCK, BLOCK), 0)
    jj = lax.broadcasted_iota(jnp.int32, (BLOCK, BLOCK), 1)
    causal = ii >= jj
    lower = jnp.where(causal, 1.0, 0.0).astype(F32)
    ld = ld_s[...]
    nt = (((1,), (1,)), ((), ()))
    by_col = lax.dot_general(lower, ld, nt, precision=lax.Precision.HIGHEST, preferred_element_type=F32)
    crow[...] = lax.dot_general(ld, lower, nt, precision=lax.Precision.HIGHEST, preferred_element_type=F32)
    for n in range(BLOCKS):
        ccol[n * BLOCK : (n + 1) * BLOCK, :] = jnp.broadcast_to(by_col[:, n : n + 1], (BLOCK, 128))

    phase("s02_kvwait")
    f_tab.wait()
    f_k.wait()
    f_v.wait()

    def rotated(ref, n):
        rows = pl.ds(pl.multiple_of(n * BLOCK, BLOCK), BLOCK)
        block = (4 * z + y) * BLOCKS + n
        cos_in, sin_in = tab_s[0], tab_s[1]
        cos_at = tab_s[2, pl.ds(block, 1), :]
        sin_at = tab_s[3, pl.ds(block, 1), :]
        cosine = cos_at * cos_in - sin_at * sin_in
        sine = sin_at * cos_in + cos_at * sin_in
        first = ref[rows, 0:HALF].astype(F32)
        second = ref[rows, HALF:DK].astype(F32)
        return rows, first * cosine - second * sine, first * sine + second * cosine

    phase("s03_states")
    s_run[...] = jnp.zeros_like(s_run)

    def state_block(n, before):
        rows, a, b = rotated(k_s, n)
        a = (a * DK**-0.5).astype(BF16)
        b = (b * DK**-0.5).astype(BF16)
        k_s[rows, 0:HALF] = a
        k_s[rows, HALF:DK] = b
        total = ccol[pl.ds(n * BLOCK + BLOCK - 1, 1), :]
        to_end = jnp.exp(total - ccol[rows, :])
        decayed = jnp.concatenate(
            [(a.astype(F32) * to_end).astype(BF16), (b.astype(F32) * to_end).astype(BF16)], axis=1
        )
        term = lax.dot_general(
            decayed, v_s[rows, :], (((0,), (0,)), ((), ())), preferred_element_type=F32
        )
        s_blk[n] = s_run[...].astype(BF16)
        s_run[...] = jnp.exp(total[:, 0:1]) * s_run[...] + term
        bstart[pl.ds(n, 1), :] = before
        return before + total

    total = lax.fori_loop(0, 4, state_block, jnp.zeros((1, 128), F32))
    phase("s03b_barrier")
    pl.semaphore_wait(barrier, 9)

    def up_at(zz, yy, half=None):
        first, size = (0, 128) if half is None else (half * 64, 64)
        return up_w.at[pl.ds(pl.multiple_of(zz * 512 + yy * 128 + first, 64), size), :]

    def dn_at(yy, zz, half=None):
        cols = pl.ds(pl.multiple_of(yy * 512 + zz * 128, 128), 128)
        return dn_w.at[:, cols] if half is None else dn_w.at[half * 512 : half * 512 + 512, cols]

    def up_own(half):
        return up_in.at[half * 64 : half * 64 + 64, :]

    def dn_own(half):
        return dn_in.at[half * 512 : half * 512 + 512, :]

    d1a = (
        net.start(dn_own(0), dn_at(y, z, 0), z=zp),
        net.start(dn_own(1), dn_at(y, z, 1), z=zm),
    )
    d1b = (
        net.start(dn_own(1), dn_at(y, z, 1), z=zp),
        net.start(dn_own(0), dn_at(y, z, 0), z=zm),
    )
    phase("s03c_states")
    total = lax.fori_loop(4, BLOCKS, state_block, total)

    phase("s04_sendstate")
    dec_tx[...] = jnp.broadcast_to(total, (8, 128))
    dec_rx[y] = jnp.broadcast_to(total, (8, 128))
    for part in range(4):
        st_tx[part] = s_run[part * QUARTER : (part + 1) * QUARTER, :].astype(BF16)
    st_copies = []
    for by in (1, 3, 2):
        to = step(y, by)
        st_copies.append(net.start(dec_tx, dec_rx.at[y], y=to))
        st_copies.append(net.start(st_tx.at[to], st_rx.at[y], y=to))
    st_rx[y] = st_tx[y]

    u1a = (
        net.start(up_own(0), up_at(z, y, 0), y=yp),
        net.start(up_own(1), up_at(z, y, 1), y=ym),
    )
    u1b = (
        net.start(up_own(1), up_at(z, y, 1), y=yp),
        net.start(up_own(0), up_at(z, y, 0), y=ym),
    )
    def arrived(*groups):
        for group in groups:
            for copy in group:
                copy.wait_recv()

    def up_out(yy):
        return (net.start(up_at(z, yy), up_at(z, yy), z=zp), net.start(up_at(z, yy), up_at(z, yy), z=zm))

    def dn_out(zz):
        return (net.start(dn_at(y, zz), dn_at(y, zz), y=yp), net.start(dn_at(y, zz), dn_at(y, zz), y=ym))

    def up_on(yy):
        return (
            net.start(up_at(zm, yy, 0), up_at(zm, yy, 0), z=zp),
            net.start(up_at(zp, yy, 1), up_at(zp, yy, 1), z=zm),
        )

    def dn_on(zz):
        return (
            net.start(dn_at(ym, zz, 0), dn_at(ym, zz, 0), y=yp),
            net.start(dn_at(yp, zz, 1), dn_at(yp, zz, 1), y=ym),
        )

    phase("s06_local1")
    f_q.wait()
    f_g.wait()

    def local_block(n, carry):
        rows, a, b = rotated(q_s, n)
        col = ccol[rows, :]
        a = a.astype(BF16)
        b = b.astype(BF16)
        query = jnp.concatenate([a, b], axis=1)
        scores = lax.dot_general(query, k_s[rows, :], nt, preferred_element_type=F32)
        spread = col - crow[pl.ds(n, 1), :]
        factor = jnp.where(causal, jnp.exp(jnp.minimum(spread, 0.0)), 0.0)
        weights = (scores * factor).astype(BF16)
        a = a.astype(F32)
        b = b.astype(F32)
        early = jnp.exp(col)
        decayed = jnp.concatenate([(a * early).astype(BF16), (b * early).astype(BF16)], axis=1)
        late = jnp.exp(col + bstart[pl.ds(n, 1), :])
        q_late[rows, 0:HALF] = (a * late).astype(BF16)
        q_late[rows, HALF:DK] = (b * late).astype(BF16)
        local[rows, :] = jnp.dot(
            weights, v_s[rows, :], preferred_element_type=F32
        ) + jnp.dot(decayed, s_blk[n], preferred_element_type=F32)
        return carry

    lax.fori_loop(0, 4, local_block, 0)

    def gate_block(n, carry):
        rows = pl.ds(pl.multiple_of(n * 64, 64), 64)
        gate = g_s[rows, :].astype(F32)
        gate_f[rows, :] = gate / (1.0 + jnp.exp(-gate))
        return carry

    lax.fori_loop(0, 16, gate_block, 0)

    phase("s07_waitstate")
    for copy in st_copies:
        copy.wait_recv()
    phase("s08_rowtotal")
    run = st_rx[0].astype(F32)
    log_row = dec_rx[0]
    for at in range(1, 4):
        run = jnp.exp(dec_rx[at][0:1, 0:1]) * run + st_rx[at].astype(F32)
        log_row = log_row + dec_rx[at]
    row_tx[...] = run.astype(BF16)
    row_rx[z] = run.astype(BF16)
    rdec_tx[...] = log_row
    rdec_rx[z] = log_row
    row_copies = []
    for by in (1, 3, 2):
        to = step(z, by)
        row_copies.append(net.start(rdec_tx, rdec_rx.at[z], z=to))
        row_copies.append(net.start(row_tx, row_rx.at[z], z=to))

    phase("s09b_w")
    arrived(d1a)
    d1c = (
        net.start(dn_at(y, zm, 0), dn_at(y, zm, 0), z=zp),
        net.start(dn_at(y, zp, 1), dn_at(y, zp, 1), z=zm),
    )
    f_up.wait()
    u2_own = up_out(y)
    phase("s09_local2")
    lax.fori_loop(4, 8, local_block, 0)
    phase("s10_waitrow")

    for copy in row_copies:
        copy.wait_recv()
    phase("s11_incoming")
    run = jnp.zeros((QUARTER, DV), F32)
    for at in range(4):
        later = jnp.exp(rdec_rx[at][0:1, 0:1]) * run + row_rx[at].astype(F32)
        run = jnp.where(at < z, later, run)
    for at in range(4):
        in_tx[at] = run.astype(BF16)
        if at < 3:
            run = jnp.exp(dec_rx[at][0:1, 0:1]) * run + st_rx[at].astype(F32)
    in_copies = []
    for by in (1, 3, 2):
        to = step(y, by)
        in_copies.append(net.start(in_tx.at[to], in_rx.at[y], y=to))
    in_rx[y] = in_tx[y]

    phase("s12_w2wait")
    arrived(u1a)
    u1c = (
        net.start(up_at(z, ym, 0), up_at(z, ym, 0), y=yp),
        net.start(up_at(z, yp, 1), up_at(z, yp, 1), y=ym),
    )
    f_dn.wait()
    d2_own = dn_out(z)
    arrived(u1b, d1b)
    u2_m, u2_p = up_out(ym), up_out(yp)
    d2_m, d2_p = dn_out(zm), dn_out(zp)

    phase("s13_waitin")
    f_wo.wait()
    f_res.wait()
    f_gain.wait()
    for copy in in_copies:
        copy.wait_recv()

    def chunk(h):
        return slice(h * 64, h * 64 + 64)

    def project(d, h):
        picks = [pl.ds(pl.multiple_of(d * 256 + i * 128 + h * 64, 64), 64) for i in range(2)]

        def both(ref):
            return jnp.concatenate([ref[rows, :] for rows in picks], axis=0)

        incoming = jnp.concatenate([in_rx[at] for at in range(4)], axis=0)
        kept = both(local) + jnp.dot(both(q_late), incoming, preferred_element_type=F32)
        scale = lax.rsqrt(jnp.mean(kept * kept, axis=-1, keepdims=True) + EPS)
        gated[...] = (both(gate_f) * kept * scale).astype(BF16)
        for j in range(4):
            part = jnp.dot(
                gated[...], wo_s[:, j * 512 : (j + 1) * 512], preferred_element_type=F32
            ).astype(BF16)
            to = slice((j % 2) * 512, (j % 2) * 512 + 512)
            p1[d, 0, j // 2, chunk(h), to] = part[0:64]
            p1[d, 1, j // 2, chunk(h), to] = part[64:128]

    def mix(d, h):
        rows = normed[d, :, chunk(h), :].reshape(128, D)
        for j in range(2):
            cols = slice(j * 512, (j + 1) * 512)
            pre = jnp.maximum(jnp.dot(rows, up_w[:, cols], preferred_element_type=F32), 0.0)
            hidden[:, cols] = (pre * pre).astype(BF16)
        for yy in range(4):
            part = jnp.dot(
                hidden[...], dn_w[:, yy * 512 : (yy + 1) * 512], preferred_element_type=F32
            ).astype(BF16)
            for zz in range(4):
                to = slice(((zz % 2) * 4 + yy) * 128, ((zz % 2) * 4 + yy) * 128 + 128)
                piece = part[:, zz * 128 : (zz + 1) * 128]
                p2[d, 0, zz // 2, chunk(h), to] = piece[0:64]
                p2[d, 1, zz // 2, chunk(h), to] = piece[64:128]

    def ring_sum(name, compute, p, p_rx, ra_p, ra_m, rb_p, rb_m):
        pairs = {}

        def add(d, h, half, extra):
            p[d, c, half, chunk(h), :] = (p[d, c, half, chunk(h), :].astype(F32) + extra.astype(F32)).astype(BF16)

        def work(key, d, h):
            phase(f"{name}{h}_work_{key}")
            compute(d, h)
            pairs[key, h] = net.start(p.at[d, other, :, chunk(h), :], p_rx.at[d, :, chunk(h), :], c=other)
            phase(f"{name}{h}_after_{key}")

        def pair_sum(key, d, h):
            phase(f"{name}{h}_pair_{key}")
            pairs[key, h].wait_recv()
            for half in range(2):
                add(d, h, half, p_rx[d, half, chunk(h), :])

        def piece(d, h, half):
            return p.at[d, c, half, chunk(h), :]

        a_copies, b_copies, c_copies = {}, {}, {}

        def send_a(h):
            a_copies[h] = (
                net.start(piece(xo, h, 0), ra_p.at[h], x=xp),
                net.start(piece(xo, h, 1), ra_m.at[h], x=xm),
            )

        def send_b(h, plus):
            if plus:
                copy = net.start(piece(xp, h, 1), rb_p.at[h, 1], x=xp)
            else:
                copy = net.start(piece(xm, h, 0), rb_m.at[h, 0], x=xm)
            b_copies[h, plus] = copy

        def send_c(h):
            phase(f"{name}{h}_wait_a")
            plus, minus = a_copies[h]
            plus.wait_recv()
            add(xp, h, 0, ra_p[h])
            first = net.start(piece(xp, h, 0), rb_p.at[h, 0], x=xp)
            minus.wait_recv()
            add(xm, h, 1, ra_m[h])
            c_copies[h] = (first, net.start(piece(xm, h, 1), rb_m.at[h, 1], x=xm))

        def complete(h):
            phase(f"{name}{h}_wait_bc")
            pairs["x", h].wait_recv()
            for copy in (b_copies[h, True], b_copies[h, False], *c_copies[h]):
                copy.wait_recv()

        work("xo", xo, 0)
        work("xp", xp, 0)
        pair_sum("xo", xo, 0)
        send_a(0)
        work("xm", xm, 0)
        pair_sum("xp", xp, 0)
        send_b(0, True)
        yield
        work("x", x, 0)
        pair_sum("xm", xm, 0)
        send_b(0, False)
        yield
        work("xo", xo, 1)
        work("xp", xp, 1)
        pair_sum("xo", xo, 1)
        send_a(1)
        work("xm", xm, 1)
        pair_sum("xp", xp, 1)
        work("x", x, 1)
        pair_sum("xm", xm, 1)
        yield
        send_c(0)
        send_b(1, True)
        send_b(1, False)
        yield
        send_c(1)
        yield
        complete(0)
        yield
        complete(1)
        yield

    def total_of(p, p_rx, rb_p, rb_m, h, half, first, size):
        rows = slice(h * 64 + first, h * 64 + first + size)
        near = slice(first, first + size)
        value = p[x, c, half, rows, :].astype(F32) + p_rx[x, half, rows, :].astype(F32)
        return value + (rb_p[h, half, near, :].astype(F32) + rb_m[h, half, near, :].astype(F32))

    def norm_chunk(h):
        phase(f"n{h}_norm")
        for first in range(0, 64, 32):
            rows = slice(h * 64 + first, h * 64 + first + 32)
            halves = []
            for half in range(2):
                cols = slice(half * 1024, (half + 1) * 1024)
                value = total_of(p1, p1_rx, rb1_p, rb1_m, h, half, first, 32)
                value = (resid_s[rows, cols].astype(F32) + value).astype(BF16)
                updated[rows, cols] = value
                halves.append(value.astype(F32))
            square = sum(jnp.sum(v * v, axis=-1, keepdims=True) for v in halves)
            scale = lax.rsqrt(square * (1.0 / D) + EPS)
            for half in range(2):
                cols = slice(half * 1024, (half + 1) * 1024)
                normed[x, c, rows, cols] = (halves[half] * scale * gain_s[:, cols]).astype(BF16)

    def share(d, first, size, **where):
        here = normed.at[d, c, first : first + size, :]
        return net.start(here, here, **where)

    def first_out(h):
        return (share(x, h * 64, 32, x=xp), share(x, h * 64 + 32, 32, x=xm))

    def rest_out(h):
        return (share(x, h * 64 + 32, 32, x=xp), share(x, h * 64, 32, x=xm))

    def pass_on(h):
        return (share(xm, h * 64, 32, x=xp), share(xp, h * 64 + 32, 32, x=xm))

    def to_pair(d, h):
        return share(d, h * 64, 64, c=other)

    ring = ring_sum("p", project, p1, p1_rx, ra1_p, ra1_m, rb1_p, rb1_m)
    next(ring)
    next(ring)
    next(ring)
    phase("w_out_far")
    arrived(u1c, d1c)
    u2_o, d2_o = up_out(step(y, 2)), dn_out(step(z, 2))
    next(ring)
    next(ring)
    phase("w_on_own")
    arrived(u2_own, d2_own)
    u3_own, d3_own = up_on(y), dn_on(z)
    next(ring)
    norm_chunk(0)
    pair_own0 = to_pair(x, 0)
    first0 = first_out(0)
    rest0 = rest_out(0)
    phase("w_on_minus")
    arrived(u2_m, d2_m)
    u3_m, d3_m = up_on(ym), dn_on(zm)
    next(ring)
    norm_chunk(1)
    pair_own1 = to_pair(x, 1)
    first1 = first_out(1)
    phase("w_on_plus")
    arrived(u2_p, d2_p)
    u3_p, d3_p = up_on(yp), dn_on(zp)
    phase("g0_wait_first")
    arrived(first0)
    on0 = pass_on(0)
    rest1 = rest_out(1)
    phase("w_on_far_u")
    arrived(u2_o)
    u3_o = up_on(step(y, 2))
    phase("g0_wait_rest")
    arrived(rest0)
    pair_near0 = (to_pair(xm, 0), to_pair(xp, 0))
    phase("w_on_far_d")
    arrived(d2_o)
    d3_o = dn_on(step(z, 2))
    phase("g1_wait_first")
    arrived(first1)
    on1 = pass_on(1)
    phase("g0_wait_on")
    arrived(on0)
    pair_far0 = to_pair(xo, 0)
    phase("g1_wait_rest")
    arrived(rest1)
    pair_near1 = (to_pair(xm, 1), to_pair(xp, 1))
    phase("w_wait")
    arrived(u3_own, u3_m, u3_p, d3_own, d3_m, d3_p, u3_o, d3_o)
    phase("g0_wait_pair")
    arrived(pair_near0, (pair_own0, pair_far0))

    ring = ring_sum("m", mix, p2, p2_rx, ra2_p, ra2_m, rb2_p, rb2_m)
    next(ring)
    phase("g1_wait_on")
    arrived(on1)
    pair_far1 = to_pair(xo, 1)
    next(ring)
    phase("g1_wait_pair")
    arrived(pair_near1, (pair_own1, pair_far1))
    for unused in range(4):
        next(ring)

    stores = []
    for h in range(2):
        if h == 1:
            next(ring)
        phase(f"f{h}_final")
        for first in range(0, 64, 32):
            rows = slice(h * 64 + first, h * 64 + first + 32)
            for half in range(2):
                cols = slice(half * 1024, (half + 1) * 1024)
                value = total_of(p2, p2_rx, rb2_p, rb2_m, h, half, first, 32)
                out_s[rows, cols] = (updated[rows, cols].astype(F32) + value).astype(BF16)
        stores.append(fetch(out_s.at[chunk(h), :], out.at[chunk(h), :]))
    phase("s35_finish")
    for copy in stores:
        copy.wait()
    net.finish()
    phase(None)


def body(resid, q, k, v, g, log_decay, wo, gain, up, dn):
    vm = pltpu.VMEM
    scratch = [
        vm((ROWS, DK), BF16), vm((ROWS, DK), BF16), vm((ROWS, DV), BF16), vm((ROWS, DV), BF16),
        vm((DV, D), BF16), vm((128, D), BF16), vm((1, D), F32), vm((BLOCKS, 128), F32),
        vm((4, 128, 128), F32),
        vm((ROWS, 128), F32), vm((BLOCKS, 128), F32), vm((BLOCKS, 128), F32),
        vm((DK, DV), F32), vm((BLOCKS, DK, DV), BF16), vm((ROWS, DV), F32), vm((ROWS, DK), BF16),
        vm((128, DV), BF16), vm((ROWS, DV), F32),
        vm((4, QUARTER, DV), BF16), vm((4, QUARTER, DV), BF16),
        vm((4, QUARTER, DV), BF16), vm((4, QUARTER, DV), BF16),
        vm((QUARTER, DV), BF16), vm((4, QUARTER, DV), BF16),
        vm((8, 128), F32), vm((4, 8, 128), F32), vm((8, 128), F32), vm((4, 8, 128), F32),
        vm((4, 2, 2, 128, 1024), BF16), vm((4, 2, 128, 1024), BF16),
        vm((2, 64, 1024), BF16), vm((2, 64, 1024), BF16),
        vm((2, 2, 64, 1024), BF16), vm((2, 2, 64, 1024), BF16),
        vm((128, D), BF16), vm((4, 2, 128, D), BF16), vm((128, FFL), BF16),
        vm((D, FFL), BF16), vm((FFL, D), BF16),
        vm((4, 2, 2, 128, 1024), BF16), vm((4, 2, 128, 1024), BF16),
        vm((2, 64, 1024), BF16), vm((2, 64, 1024), BF16),
        vm((2, 2, 64, 1024), BF16), vm((2, 2, 64, 1024), BF16),
        vm((128, D), BF16),
        pltpu.SemaphoreType.DMA((N_COPIES,)),
        pltpu.SemaphoreType.DMA((N_COPIES,)),
        pltpu.SemaphoreType.DMA((N_LOCAL,)),
    ]
    anywhere = pl.BlockSpec(memory_space=pl.ANY)
    return pl.pallas_call(
        kernel,
        out_shape=jax.ShapeDtypeStruct((128, D), BF16),
        in_specs=[anywhere] * 11,
        out_specs=anywhere,
        scratch_shapes=scratch,
        compiler_params=pltpu.CompilerParams(
            collective_id=0, has_side_effects=True, vmem_limit_bytes=66_000_000
        ),
    )(
        resid, q, k, v, g, log_decay.reshape(BLOCKS, BLOCK), wo,
        gain.astype(F32).reshape(1, D), up, dn, jnp.asarray(rotation_tables()),
    )


def solution(mesh):
    torus = Mesh(mesh.devices.reshape(4, 4, 4, 2), ("z", "y", "x", "c"))
    sp, tp = ("z", "y"), ("x", "c")
    placed = (
        P(("z", "y", "x", "c"), None),
        P(sp, tp),
        P(sp, tp),
        P(sp, tp),
        P(sp, tp),
        P(tp, sp),
        P(tp, None),
        P(),
        P(sp, tp),
        P(tp, sp),
    )
    return jax.shard_map(
        body, mesh=torus, in_specs=placed, out_specs=P(("z", "y", "x", "c"), None), check_vma=False
    )
```

time: 105 us -> 91.4 us (0.87)
  Pallas kernels: 102 us -> 88 us
    pallas_call x1, Pallas kernels: 102 us -> 88 us  [body(): pl.pallas_call(kernel, out_shape=jax.ShapeDtypeStruct((128, D), BF16), in...]
where the time goes in v2:
time: 91.4 us; the launch traced here: 91.2 us
  Pallas kernels  88 us (96%)
  local copies, waits for them, and re-layouts  1.88 us (2%)
  other arithmetic  1.29 us (1%)
    pallas_call x1, Pallas kernels, body(): pl.pallas_call(kernel, out_shape=jax.ShapeDtypeStruct((128, D), BF16), in...  88 us
    unnamed x1, local copies, waits for them, and re-layouts  1.88 us

profile of v2, /device:TPU:1, one launch (start us, length us, event | category | flops | bytes accessed | tf_op | source)
XLA Modules:
  0.0 91.2 jit_solution(4753810806132099847)
XLA Ops:
  0.0 1.3 %reshape.11 = f32[2048]{0:T(1024)} convert(bf16[2048]{0:T(1024)(128)(2,1)} %param.18) | non-fusion elementwise | flops 2048 | bytes 12288 | tf_op jit(solution)/shard_map/reshape | solution.py:635
  1.3 88.0 %shard_map.109 = bf16[128,2048]{1,0:T(8,128)(2,1)} custom-call(bf16[128,2048]{1,0:T(8,128)(2,1)} %resid.1, bf16[1024,256]{1,0:T(8,128)(2,1)} %q_in.1, bf16[1024,256]{1,0:T(8,128)(2,1)} %k_in.1, bf16[1024,512]{1,0:T(8,128)(2,1)} %v_in.1, bf16[1024,512]{1,0:T(8,128)(2,1)} %g_in.1, f32[8,128]{1,0:T(8,128)} %bitcast.3, bf16[512,2048]{1,0:T(8,128)(2,1)} %wo_in.1, ...), custom_call_target="tpu_custom_call" | custom-call | tf_op jit(solution)/shard_map/pallas_call | solution.py:624
  89.3 1.9 %copy.13 = bf16[128,2048]{1,0:T(8,128)(2,1)} copy(bf16[128,2048]{1,0:T(8,128)(2,1)} %shard_map.109) | data formatting | bytes 1048576

commit v3 on v2

v3 whole, which is shorter than its diff:
```python
import jax
import jax.numpy as jnp
import numpy as np
from jax import lax
from jax.experimental import pallas as pl
from jax.experimental.pallas import tpu as pltpu
from jax.sharding import Mesh
from jax.sharding import PartitionSpec as P

DK = 256
DV = 512
HALF = DK // 2
BLOCK = 128
BLOCKS = 8
ROWS = 1024
D = 2048
FFL = 1024
QUARTER = DK // 4
EPS = 1e-06
F32 = jnp.float32
BF16 = jnp.bfloat16


def rotation_tables():
    inverse = 10000.0 ** (-np.arange(0, DK, 2, dtype=np.float64) / DK)
    inside = np.arange(BLOCK, dtype=np.float64)[:, None] * inverse[None, :]
    start = (np.arange(128, dtype=np.float64) * BLOCK)[:, None] * inverse[None, :]
    return np.stack([np.cos(inside), np.sin(inside), np.cos(start), np.sin(start)]).astype(np.float32)


class Phases:
    def __init__(self):
        self.scope = None

    def __call__(self, name):
        if self.scope is not None:
            self.scope.__exit__(None, None, None)
        self.scope = None
        if name is not None:
            self.scope = jax.named_scope(name)
            self.scope.__enter__()


class Copies:
    def __init__(self, send, recv, local, sized):
        self.send, self.recv, self.local, self.sized = send, recv, local, sized
        self.count = self.local_count = 0
        self.sent = {}

    def group(self):
        self.count += 1
        return Group(self, self.recv.at[self.count - 1])

    def start(self, kind, group, src, dst, **where):
        at, size = self.sent.get(kind, (len(self.sent), 0))
        self.sent[kind] = (at, size + bytes_of(src))
        group.size += bytes_of(dst)
        pltpu.make_async_remote_copy(
            src_ref=src,
            dst_ref=dst,
            send_sem=self.send.at[at],
            recv_sem=group.sem,
            device_id=where,
            device_id_type=pl.DeviceIdType.MESH,
        ).start()

    def local_copies(self, *pairs):
        self.local_count += 1
        group = Group(self, self.local.at[self.local_count - 1])
        for src, dst in pairs:
            pltpu.make_async_copy(src, dst, group.sem).start()
            group.size += bytes_of(dst)
        return group

    def finish(self):
        for at, size in self.sent.values():
            view = self.sized(size)
            pltpu.make_async_copy(view, view, self.send.at[at]).wait()


class Group:
    def __init__(self, net, sem):
        self.net, self.sem, self.size = net, sem, 0

    def wait(self):
        view = self.net.sized(self.size)
        pltpu.make_async_copy(view, view, self.sem).wait()


def bytes_of(ref):
    return int(np.prod(ref.shape)) * jnp.dtype(ref.dtype).itemsize


N_SEND = 7
N_RECV = 56
N_LOCAL = 8


def kernel(
    resid, q_in, k_in, v_in, g_in, ld_in, wo_in, gain_in, up_in, dn_in, tab_in, out,
    q_s, k_s, v_s, g_s, wo_s, resid_s, gain_s, ld_s, tab_s,
    ccol, crow, bstart, s_run, s_blk, local, q_late, gated, gate_f,
    st_tx, st_rx, in_tx, in_rx, row_tx, row_rx, dec_tx, dec_rx, rdec_tx, rdec_rx,
    p1, p1_rx, ra1, rb1,
    updated, normed, hidden, up_w, dn_w,
    p2, p2_rx, ra2, rb2, p3, p3_rx, ra3, rb3, out_s,
    send, recv, loc,
):
    z, y = lax.axis_index("z"), lax.axis_index("y")
    x, c = lax.axis_index("x"), lax.axis_index("c")

    def step(a, by):
        return lax.rem(a + by, 4)

    xp, xm, xo = step(x, 1), step(x, 3), step(x, 2)
    yp, ym = step(y, 1), step(y, 3)
    zp, zm = step(z, 1), step(z, 3)
    other = 1 - c
    def sized(size):
        if size % 32768 == 0:
            return up_w.at[0 : size // 2048, :]
        return tab_s.at[0, 0 : size // 512, :]

    net = Copies(send, recv, loc, sized)
    phase = Phases()
    phase("s00_barrier")

    own_rows = pl.ds(pl.multiple_of((4 * z + y) * 128, 128), 128)
    own_cols = pl.ds(pl.multiple_of((4 * y + z) * 128, 128), 128)

    barrier = pltpu.get_barrier_semaphore()
    for where in (
        {"y": yp}, {"y": ym}, {"y": step(y, 2)},
        {"z": zp}, {"z": zm}, {"z": step(z, 2)},
        {"x": xp}, {"x": xm}, {"c": other},
    ):
        pl.semaphore_signal(barrier, inc=1, device_id=where, device_id_type=pl.DeviceIdType.MESH)

    f_ld = net.local_copies((ld_in, ld_s))
    f_kv = net.local_copies((tab_in, tab_s), (k_in, k_s), (v_in, v_s))
    f_qg = net.local_copies((q_in, q_s), (g_in, g_s))
    f_wo = net.local_copies((wo_in, wo_s), (resid, resid_s))
    f_gain = net.local_copies((gain_in, gain_s))
    f_up = net.local_copies((up_in, up_w.at[own_rows, :]))
    f_dn = net.local_copies((dn_in, dn_w.at[:, own_cols]))

    phase("s01_decays")
    f_ld.wait()
    ii = lax.broadcasted_iota(jnp.int32, (BLOCK, BLOCK), 0)
    jj = lax.broadcasted_iota(jnp.int32, (BLOCK, BLOCK), 1)
    causal = ii >= jj
    lower = jnp.where(causal, 1.0, 0.0).astype(F32)
    ld = ld_s[...]
    nt = (((1,), (1,)), ((), ()))
    by_col = lax.dot_general(lower, ld, nt, precision=lax.Precision.HIGHEST, preferred_element_type=F32)
    crow[...] = lax.dot_general(ld, lower, nt, precision=lax.Precision.HIGHEST, preferred_element_type=F32)
    for n in range(BLOCKS):
        ccol[n * BLOCK : (n + 1) * BLOCK, :] = jnp.broadcast_to(by_col[:, n : n + 1], (BLOCK, 128))

    phase("s02_kvwait")
    whole = sum(ccol[n * BLOCK + BLOCK - 1 : (n + 1) * BLOCK, :] for n in range(BLOCKS))
    dec_tx[...] = jnp.broadcast_to(whole, (8, 128))
    dec_rx[y] = jnp.broadcast_to(whole, (8, 128))

    f_kv.wait()

    def rotated(ref, n):
        rows = pl.ds(pl.multiple_of(n * BLOCK, BLOCK), BLOCK)
        block = (4 * z + y) * BLOCKS + n
        cos_in, sin_in = tab_s[0], tab_s[1]
        cos_at = tab_s[2, pl.ds(block, 1), :]
        sin_at = tab_s[3, pl.ds(block, 1), :]
        cosine = cos_at * cos_in - sin_at * sin_in
        sine = sin_at * cos_in + cos_at * sin_in
        first = ref[rows, 0:HALF].astype(F32)
        second = ref[rows, HALF:DK].astype(F32)
        return rows, first * cosine - second * sine, first * sine + second * cosine

    phase("s03_states")
    s_run[...] = jnp.zeros_like(s_run)

    def state_block(n, before):
        rows, a, b = rotated(k_s, n)
        a = (a * DK**-0.5).astype(BF16)
        b = (b * DK**-0.5).astype(BF16)
        k_s[rows, 0:HALF] = a
        k_s[rows, HALF:DK] = b
        total = ccol[pl.ds(n * BLOCK + BLOCK - 1, 1), :]
        to_end = jnp.exp(total - ccol[rows, :])
        decayed = jnp.concatenate(
            [(a.astype(F32) * to_end).astype(BF16), (b.astype(F32) * to_end).astype(BF16)], axis=1
        )
        term = lax.dot_general(
            decayed, v_s[rows, :], (((0,), (0,)), ((), ())), preferred_element_type=F32
        )
        s_blk[n] = s_run[...].astype(BF16)
        s_run[...] = jnp.exp(total[:, 0:1]) * s_run[...] + term
        bstart[pl.ds(n, 1), :] = before
        return before + total

    total = lax.fori_loop(0, 4, state_block, jnp.zeros((1, 128), F32), unroll=True)
    phase("s03b_barrier")
    pl.semaphore_wait(barrier, 9)
    dec_copies = net.group()
    for by in (2, 1, 3):
        net.start("decay", dec_copies, dec_tx, dec_rx.at[y], y=step(y, by))

    def up_at(zz, yy, half=None):
        first, size = (0, 128) if half is None else (half * 64, 64)
        return up_w.at[pl.ds(pl.multiple_of(zz * 512 + yy * 128 + first, 64), size), :]

    def dn_at(yy, zz, half=None):
        cols = pl.ds(pl.multiple_of(yy * 512 + zz * 128, 128), 128)
        return dn_w.at[:, cols] if half is None else dn_w.at[half * 512 : half * 512 + 512, cols]

    def up_own(half):
        return up_in.at[half * 64 : half * 64 + 64, :]

    def dn_own(half):
        return dn_in.at[half * 512 : half * 512 + 512, :]

    def two(kind, axis, plus, minus, group=None):
        group = net.group() if group is None else group
        ahead, behind = {"x": (xp, xm), "y": (yp, ym), "z": (zp, zm)}[axis]
        for to, (src, dst) in ((ahead, plus), (behind, minus)):
            net.start(kind, group, src, dst, **{axis: to})
        return group

    d1a = two("down", "z", (dn_own(0), dn_at(y, z, 0)), (dn_own(1), dn_at(y, z, 1)))
    d1b = two("down", "z", (dn_own(1), dn_at(y, z, 1)), (dn_own(0), dn_at(y, z, 0)))
    phase("s03c_states")
    lax.fori_loop(4, BLOCKS, state_block, total, unroll=True)

    phase("s04_sendstate")
    for part in range(4):
        st_tx[part] = s_run[part * QUARTER : (part + 1) * QUARTER, :].astype(BF16)
    st_copies = net.group()
    for by in (2, 1, 3):
        to = step(y, by)
        net.start("state", st_copies, st_tx.at[to], st_rx.at[y], y=to)
    st_rx[y] = st_tx[y]

    def arrived(*groups):
        for group in groups:
            group.wait()

    def twice(ref):
        return ref, ref

    def up_out(yy):
        return two("up", "z", twice(up_at(z, yy)), twice(up_at(z, yy)))

    def dn_out(zz):
        return two("down", "y", twice(dn_at(y, zz)), twice(dn_at(y, zz)))

    def up_on(*ys):
        for yy in ys:
            two("up", "z", twice(up_at(zm, yy, 0)), twice(up_at(zp, yy, 1)), up_last)

    def dn_on(*zs):
        for zz in zs:
            two("down", "y", twice(dn_at(ym, zz, 0)), twice(dn_at(yp, zz, 1)), dn_last)

    up_last, dn_last = net.group(), net.group()

    phase("s06_local1")
    f_qg.wait()

    def local_block(n, carry):
        rows, a, b = rotated(q_s, n)
        col = ccol[rows, :]
        a = a.astype(BF16)
        b = b.astype(BF16)
        query = jnp.concatenate([a, b], axis=1)
        scores = lax.dot_general(query, k_s[rows, :], nt, preferred_element_type=F32)
        spread = col - crow[pl.ds(n, 1), :]
        factor = jnp.where(causal, jnp.exp(jnp.minimum(spread, 0.0)), 0.0)
        weights = (scores * factor).astype(BF16)
        a = a.astype(F32)
        b = b.astype(F32)
        early = jnp.exp(col)
        decayed = jnp.concatenate([(a * early).astype(BF16), (b * early).astype(BF16)], axis=1)
        late = jnp.exp(col + bstart[pl.ds(n, 1), :])
        q_late[rows, 0:HALF] = (a * late).astype(BF16)
        q_late[rows, HALF:DK] = (b * late).astype(BF16)
        local[rows, :] = jnp.dot(
            weights, v_s[rows, :], preferred_element_type=F32
        ) + jnp.dot(decayed, s_blk[n], preferred_element_type=F32)
        return carry

    lax.fori_loop(0, 4, local_block, 0)

    dec_copies.wait()
    log_row = dec_rx[0] + dec_rx[1] + dec_rx[2] + dec_rx[3]
    rdec_tx[...] = log_row
    rdec_rx[z] = log_row
    rdec_copies = net.group()
    for by in (2, 1, 3):
        net.start("decay", rdec_copies, rdec_tx, rdec_rx.at[z], z=step(z, by))

    def gate_block(n, carry):
        rows = pl.ds(pl.multiple_of(n * 64, 64), 64)
        gate = g_s[rows, :].astype(F32)
        gate_f[rows, :] = gate / (1.0 + jnp.exp(-gate))
        return carry

    lax.fori_loop(0, 16, gate_block, 0)
    u1a = two("up", "y", (up_own(0), up_at(z, y, 0)), (up_own(1), up_at(z, y, 1)))

    phase("s07_waitstate")
    st_copies.wait()
    phase("s08_rowtotal")
    run = st_rx[0].astype(F32)
    for at in range(1, 4):
        run = jnp.exp(dec_rx[at][0:1, 0:1]) * run + st_rx[at].astype(F32)
    row_tx[...] = run.astype(BF16)
    row_rx[z] = run.astype(BF16)
    row_copies = net.group()
    for by in (2, 1, 3):
        net.start("state", row_copies, row_tx, row_rx.at[z], z=step(z, by))

    u1b = two("up", "y", (up_own(1), up_at(z, y, 1)), (up_own(0), up_at(z, y, 0)))
    phase("s09b_w")
    arrived(d1a)
    d1c = two("down", "z", twice(dn_at(y, zm, 0)), twice(dn_at(y, zp, 1)))
    f_up.wait()
    u2_own = up_out(y)
    phase("s09_local2")
    lax.fori_loop(4, 8, local_block, 0)
    phase("s10_waitrow")

    rdec_copies.wait()
    row_copies.wait()
    phase("s11_incoming")
    run = jnp.zeros((QUARTER, DV), F32)
    for at in range(4):
        later = jnp.exp(rdec_rx[at][0:1, 0:1]) * run + row_rx[at].astype(F32)
        run = jnp.where(at < z, later, run)
    for at in range(4):
        in_tx[at] = run.astype(BF16)
        if at < 3:
            run = jnp.exp(dec_rx[at][0:1, 0:1]) * run + st_rx[at].astype(F32)
    in_copies = net.group()
    for by in (2, 1, 3):
        to = step(y, by)
        net.start("state", in_copies, in_tx.at[to], in_rx.at[y], y=to)
    in_rx[y] = in_tx[y]

    phase("s13_waitin")
    f_wo.wait()
    f_gain.wait()
    in_copies.wait()
    phase("s12_w2wait")
    arrived(u1a)
    u1c = two("up", "y", twice(up_at(z, ym, 0)), twice(up_at(z, yp, 1)))
    f_dn.wait()
    d2_own = dn_out(z)
    arrived(u1b, d1b)
    u2_m, u2_p = up_out(ym), up_out(yp)
    d2_m, d2_p = dn_out(zm), dn_out(zp)
    def chunk(h):
        return slice(h * 64, h * 64 + 64)

    def project(d, h):
        picks = [pl.ds(pl.multiple_of(d * 256 + i * 128 + h * 64, 64), 64) for i in range(2)]

        def both(ref):
            return jnp.concatenate([ref[rows, :] for rows in picks], axis=0)

        incoming = jnp.concatenate([in_rx[at] for at in range(4)], axis=0)
        kept = both(local) + jnp.dot(both(q_late), incoming, preferred_element_type=F32)
        scale = lax.rsqrt(jnp.mean(kept * kept, axis=-1, keepdims=True) + EPS)
        gated[...] = (both(gate_f) * kept * scale).astype(BF16)
        for j in range(4):
            part = jnp.dot(
                gated[...], wo_s[:, j * 512 : (j + 1) * 512], preferred_element_type=F32
            ).astype(BF16)
            to = slice((j % 2) * 512, (j % 2) * 512 + 512)
            p1[h, d, 0, j // 2, :, to] = part[0:64]
            p1[h, d, 1, j // 2, :, to] = part[64:128]

    def mix_up(d, h):
        rows = normed[d, :, chunk(h), :].reshape(128, D)
        for j in range(2):
            cols = slice(j * 512, (j + 1) * 512)
            pre = jnp.maximum(jnp.dot(rows, up_w[:, cols], preferred_element_type=F32), 0.0)
            hidden[d, h, :, cols] = (pre * pre).astype(BF16)

    order = (y, ym, yp, step(y, 2))

    def dn_cols(k):
        return dn_w[:, pl.ds(pl.multiple_of(order[k] * 512, 512), 512)]

    def mix_down(d, h):
        for k in range(3):
            part = jnp.dot(hidden[d, h], dn_cols(k), preferred_element_type=F32).astype(BF16)
            for core in range(2):
                rows = slice(core * 64, core * 64 + 64)
                for at in range(0, 512, 256):
                    col = k * 512 + at
                    p2[h, d, core, col // 768, :, col % 768 : col % 768 + 256] = part[rows, at : at + 256]

    def mix_last(d, unused):
        part = jnp.dot(
            hidden[d].reshape(256, FFL), dn_cols(3), preferred_element_type=F32
        ).astype(BF16)
        for h in range(2):
            for core in range(2):
                at = h * 128 + core * 64
                for half in range(2):
                    p3[d, core, half, chunk(h), :] = part[at : at + 64, half * 256 : half * 256 + 256]

    class RingSum:
        blocks = {"xo": xo, "xp": xp, "xm": xm, "x": x}

        def __init__(self, name, compute, arg, p, p_rx, ra, rb):
            self.name, self.compute, self.arg = name, compute, arg
            self.p, self.p_rx = p, p_rx
            self.ra_p, self.ra_m, self.rb_p, self.rb_m = ra.at[0], ra.at[1], rb.at[0], rb.at[1]
            self.pairs, self.a, self.done = {}, net.group(), net.group()
            self.kind = name[0]

        def add(self, d, half, extra):
            total = self.p[d, c, half].astype(F32) + extra.astype(F32)
            self.p[d, c, half] = total.astype(BF16)

        def work(self, *keys):
            for key in keys:
                phase(f"{self.name}_work_{key}")
                d = self.blocks[key]
                self.compute(d, self.arg)
                self.pairs[key] = self.done if key == "x" else net.group()
                net.start(self.kind, self.pairs[key], self.p.at[d, other], self.p_rx.at[d], c=other)

        def pair_sum(self, key):
            phase(f"{self.name}_pair_{key}")
            d = self.blocks[key]
            self.pairs[key].wait()
            for half in range(2):
                self.add(d, half, self.p_rx[d, half])

        def piece(self, d, half):
            return self.p.at[d, c, half]

        def send(self, group, src, dst, to):
            net.start(self.kind, group, src, dst, x=to)

        def send_a(self):
            self.pair_sum("xo")
            self.send(self.a, self.piece(xo, 0), self.ra_p, xp)
            self.send(self.a, self.piece(xo, 1), self.ra_m, xm)

        def send_b(self):
            self.pair_sum("xp")
            self.send(self.done, self.piece(xp, 1), self.rb_p.at[1], xp)
            self.pair_sum("xm")
            self.send(self.done, self.piece(xm, 0), self.rb_m.at[0], xm)

        def send_c(self):
            phase(f"{self.name}_wait_a")
            self.a.wait()
            self.add(xp, 0, self.ra_p[...])
            self.send(self.done, self.piece(xp, 0), self.rb_p.at[0], xp)
            self.add(xm, 1, self.ra_m[...])
            self.send(self.done, self.piece(xm, 1), self.rb_m.at[1], xm)

        def complete(self):
            phase(f"{self.name}_wait_bc")
            self.done.wait()

        def total(self, half, rows, cols):
            value = self.p[x, c, half, rows, cols].astype(F32) + self.p_rx[x, half, rows, cols].astype(F32)
            sides = self.rb_p[half, rows, cols].astype(F32) + self.rb_m[half, rows, cols].astype(F32)
            return value + sides

    rings1 = [RingSum(f"p{h}", project, h, p1.at[h], p1_rx.at[h], ra1.at[h], rb1.at[h]) for h in range(2)]

    def norm_chunk(h):
        phase(f"n{h}_norm")
        gain = gain_s[...].astype(F32).reshape(1, D)
        for first in range(0, 64, 32):
            rows = slice(h * 64 + first, h * 64 + first + 32)
            halves = []
            for half in range(2):
                cols = slice(half * 1024, (half + 1) * 1024)
                value = rings1[h].total(half, slice(first, first + 32), slice(None))
                value = (resid_s[rows, cols].astype(F32) + value).astype(BF16)
                updated[rows, cols] = value
                halves.append(value.astype(F32))
            square = sum(jnp.sum(v * v, axis=-1, keepdims=True) for v in halves)
            scale = lax.rsqrt(square * (1.0 / D) + EPS)
            for half in range(2):
                cols = slice(half * 1024, (half + 1) * 1024)
                normed[x, c, rows, cols] = (halves[half] * scale * gain[:, cols]).astype(BF16)

    def rows_at(d, first, size):
        return twice(normed.at[d, c, first : first + size, :])

    def first_out(h):
        return two("gather", "x", rows_at(x, h * 64, 32), rows_at(x, h * 64 + 32, 32))

    def rest_out(h):
        return two("gather", "x", rows_at(x, h * 64 + 32, 32), rows_at(x, h * 64, 32))

    def pass_on(h):
        return two("gather", "x", rows_at(xm, h * 64, 32), rows_at(xp, h * 64 + 32, 32))

    def to_pair(d, h, group):
        net.start("gather", group, *rows_at(d, h * 64, 64), c=other)

    near = [net.group() for h in range(2)]
    far = [net.group() for h in range(2)]

    r0, r1 = rings1
    r0.work("xo", "xp")
    r0.send_a()
    r0.work("xm")
    r1.work("xo")
    r0.send_b()
    r1.work("xp")
    r1.send_a()
    r1.work("xm", "x")
    r0.work("x")
    phase("w_out_far")
    arrived(u1c, d1c)
    u2_o, d2_o = up_out(step(y, 2)), dn_out(step(z, 2))
    r0.send_c()
    r1.send_b()
    r1.send_c()
    phase("w_on_own")
    arrived(u2_own, d2_own)
    up_on(y)
    dn_on(z)
    r0.complete()
    norm_chunk(0)
    to_pair(x, 0, near[0])
    first0 = first_out(0)
    rest0 = rest_out(0)
    phase("w_on_minus")
    arrived(u2_m, d2_m)
    up_on(ym)
    dn_on(zm)
    r1.complete()
    norm_chunk(1)
    to_pair(x, 1, near[1])
    first1 = first_out(1)
    rest1 = rest_out(1)
    phase("w_on_plus")
    arrived(u2_p, d2_p)
    up_on(yp)
    dn_on(zp)
    phase("g0_wait_first")
    arrived(first0)
    on0 = pass_on(0)
    phase("w_on_far_u")
    arrived(u2_o)
    up_on(step(y, 2))
    phase("g0_wait_rest")
    arrived(rest0)
    for d in (xm, xp):
        to_pair(d, 0, near[0])
    phase("w_on_far_d")
    arrived(d2_o)
    dn_on(step(z, 2))
    phase("g1_wait_first")
    arrived(first1)
    on1 = pass_on(1)
    phase("g0_wait_pair")
    arrived(near[0])
    phase("w_wait_up")
    arrived(up_last)

    r0, r1 = [
        RingSum(f"m{h}", mix_down, h, p2.at[h], p2_rx.at[h], ra2.at[h], rb2.at[h]) for h in range(2)
    ]
    r2 = RingSum("m2", mix_last, None, p3, p3_rx, ra3, rb3)
    phase("m0_up_near")
    mix_up(xp, 0)
    mix_up(xm, 0)
    phase("g1_wait_rest")
    arrived(rest1)
    for d in (xm, xp):
        to_pair(d, 1, near[1])
    r0.work("xp", "xm")
    phase("g0_wait_on")
    arrived(on0)
    to_pair(xo, 0, far[0])
    phase("g1_wait_pair")
    arrived(near[1])
    phase("m1_up_near")
    mix_up(xp, 1)
    mix_up(xm, 1)
    r0.send_b()
    r1.work("xp", "xm")
    phase("g0_wait_far")
    arrived(far[0])
    phase("m0_up_far")
    mix_up(xo, 0)
    r0.work("xo")
    r1.send_b()
    phase("g1_wait_on")
    arrived(on1)
    to_pair(xo, 1, far[1])
    phase("m0_up_own")
    mix_up(x, 0)
    r0.send_a()
    phase("m1_up_own")
    mix_up(x, 1)
    phase("g1_wait_far")
    arrived(far[1])
    phase("m1_up_far")
    mix_up(xo, 1)
    r1.work("xo")
    phase("w_wait_last")
    arrived(dn_last)
    r2.work("xo")
    r1.send_a()
    r2.work("xp")
    r2.send_a()
    r0.send_c()
    r2.work("xm")
    r1.send_c()
    r2.send_b()
    r0.work("x")
    r1.work("x")
    r2.work("x")
    r2.send_c()

    def finish_columns(k, rows, total_at):
        for zz in range(4):
            cols = pl.ds(pl.multiple_of((4 * zz + order[k]) * 128, 128), 128)
            out_s[rows, cols] = (updated[rows, cols].astype(F32) + total_at(zz * 128)).astype(BF16)

    def chunk_total(ring, k):
        def at(first):
            col = k * 512 + first
            return ring.total(col // 768, slice(None), slice(col % 768, col % 768 + 128))

        return at

    for h, ring in enumerate((r0, r1)):
        ring.complete()
        phase(f"f{h}_final")
        for k in range(3):
            finish_columns(k, chunk(h), chunk_total(ring, k))
    r2.complete()
    phase("f2_final")
    finish_columns(3, slice(None), lambda first: r2.total(first // 256, slice(None), slice(first % 256, first % 256 + 128)))
    store = net.local_copies((out_s, out))
    phase("s35_finish")
    store.wait()
    net.finish()
    phase(None)


def body(resid, q, k, v, g, log_decay, wo, gain, up, dn):
    vm = pltpu.VMEM
    scratch = [
        vm((ROWS, DK), BF16), vm((ROWS, DK), BF16), vm((ROWS, DV), BF16), vm((ROWS, DV), BF16),
        vm((DV, D), BF16), vm((128, D), BF16), vm((D,), BF16), vm((BLOCKS, 128), F32),
        vm((4, 128, 128), F32),
        vm((ROWS, 128), F32), vm((BLOCKS, 128), F32), vm((BLOCKS, 128), F32),
        vm((DK, DV), F32), vm((BLOCKS, DK, DV), BF16), vm((ROWS, DV), F32), vm((ROWS, DK), BF16),
        vm((128, DV), BF16), vm((ROWS, DV), F32),
        vm((4, QUARTER, DV), BF16), vm((4, QUARTER, DV), BF16),
        vm((4, QUARTER, DV), BF16), vm((4, QUARTER, DV), BF16),
        vm((QUARTER, DV), BF16), vm((4, QUARTER, DV), BF16),
        vm((8, 128), F32), vm((4, 8, 128), F32), vm((8, 128), F32), vm((4, 8, 128), F32),
        vm((2, 4, 2, 2, 64, 1024), BF16), vm((2, 4, 2, 64, 1024), BF16),
        vm((2, 2, 64, 1024), BF16), vm((2, 2, 2, 64, 1024), BF16),
        vm((128, D), BF16), vm((4, 2, 128, D), BF16), vm((4, 2, 128, FFL), BF16),
        vm((D, FFL), BF16), vm((FFL, D), BF16),
        vm((2, 4, 2, 2, 64, 768), BF16), vm((2, 4, 2, 64, 768), BF16),
        vm((2, 2, 64, 768), BF16), vm((2, 2, 2, 64, 768), BF16),
        vm((4, 2, 2, 128, 256), BF16), vm((4, 2, 128, 256), BF16),
        vm((2, 128, 256), BF16), vm((2, 2, 128, 256), BF16),
        vm((128, D), BF16),
        pltpu.SemaphoreType.DMA((N_SEND,)),
        pltpu.SemaphoreType.DMA((N_RECV,)),
        pltpu.SemaphoreType.DMA((N_LOCAL,)),
    ]
    anywhere = pl.BlockSpec(memory_space=pl.ANY)
    return pl.pallas_call(
        kernel,
        out_shape=jax.ShapeDtypeStruct((128, D), BF16),
        in_specs=[anywhere] * 11,
        out_specs=anywhere,
        scratch_shapes=scratch,
        compiler_params=pltpu.CompilerParams(
            collective_id=0, has_side_effects=True, vmem_limit_bytes=66_000_000
        ),
    )(
        resid, q, k, v, g, log_decay.reshape(BLOCKS, BLOCK), wo,
        gain, up, dn, jnp.asarray(rotation_tables()),
    )


def solution(mesh):
    torus = Mesh(mesh.devices.reshape(4, 4, 4, 2), ("z", "y", "x", "c"))
    sp, tp = ("z", "y"), ("x", "c")
    placed = (
        P(("z", "y", "x", "c"), None),
        P(sp, tp),
        P(sp, tp),
        P(sp, tp),
        P(sp, tp),
        P(tp, sp),
        P(tp, None),
        P(),
        P(sp, tp),
        P(tp, sp),
    )
    return jax.shard_map(
        body, mesh=torus, in_specs=placed, out_specs=P(("z", "y", "x", "c"), None), check_vma=False
    )
```

time: 91.4 us -> 85.5 us (0.935)
  Pallas kernels: 88 us -> 83.5 us
  other arithmetic: 1.29 us -> 0 us
    pallas_call x1, Pallas kernels: 88 us -> 83.5 us  [body(): pl.pallas_call(kernel, out_shape=jax.ShapeDtypeStruct((128, D), BF16), in...]
    reshape x1 -> x0, other arithmetic: 1.29 us -> none  [body(): gain.astype(F32).reshape(1, D)]
where the time goes in v3:
time: 85.5 us; the launch traced here: 85.3 us
  Pallas kernels  83.5 us (98%)
  local copies, waits for them, and re-layouts  1.88 us (2%)
    pallas_call x1, Pallas kernels, body(): pl.pallas_call(kernel, out_shape=jax.ShapeDtypeStruct((128, D), BF16), in...  83.5 us
    unnamed x1, local copies, waits for them, and re-layouts  1.88 us

profile of v3, /device:TPU:1, one launch (start us, length us, event | category | flops | bytes accessed | tf_op | source)
XLA Modules:
  0.0 85.3 jit_solution(4124180561890182974)
XLA Ops:
  0.0 83.5 %shard_map.109 = bf16[128,2048]{1,0:T(8,128)(2,1)} custom-call(bf16[128,2048]{1,0:T(8,128)(2,1)} %resid.1, bf16[1024,256]{1,0:T(8,128)(2,1)} %q_in.1, bf16[1024,256]{1,0:T(8,128)(2,1)} %k_in.1, bf16[1024,512]{1,0:T(8,128)(2,1)} %v_in.1, bf16[1024,512]{1,0:T(8,128)(2,1)} %g_in.1, f32[8,128]{1,0:T(8,128)} %bitcast.1, bf16[512,2048]{1,0:T(8,128)(2,1)} %wo_in.1, ...), custom_call_target="tpu_custom_call" | custom-call | tf_op jit(solution)/shard_map/pallas_call | solution.py:683
  83.5 1.9 %copy.13 = bf16[128,2048]{1,0:T(8,128)(2,1)} copy(bf16[128,2048]{1,0:T(8,128)(2,1)} %shard_map.109) | data formatting | bytes 1048576

commit v4 on v3

--- a/solution.py
+++ b/solution.py
@@ -52,8 +52,11 @@
         return Group(self, self.recv.at[self.count - 1])
 
     def start(self, kind, group, src, dst, **where):
-        at, size = self.sent.get(kind, (len(self.sent), 0))
-        self.sent[kind] = (at, size + bytes_of(src))
+        if kind is None:
+            at = N_SEND - 1
+        else:
+            at, size = self.sent.get(kind, (len(self.sent), 0))
+            self.sent[kind] = (at, size + bytes_of(src))
         group.size += bytes_of(dst)
         pltpu.make_async_remote_copy(
             src_ref=src,
@@ -82,8 +85,8 @@
     def __init__(self, net, sem):
         self.net, self.sem, self.size = net, sem, 0
 
-    def wait(self):
-        view = self.net.sized(self.size)
+    def wait(self, size=None):
+        view = self.net.sized(self.size if size is None else size)
         pltpu.make_async_copy(view, view, self.sem).wait()
 
 
@@ -91,7 +94,7 @@
     return int(np.prod(ref.shape)) * jnp.dtype(ref.dtype).itemsize
 
 
-N_SEND = 7
+N_SEND = 8
 N_RECV = 56
 N_LOCAL = 8
 
@@ -314,10 +317,13 @@
     for at in range(1, 4):
         run = jnp.exp(dec_rx[at][0:1, 0:1]) * run + st_rx[at].astype(F32)
     row_tx[...] = run.astype(BF16)
-    row_rx[z] = run.astype(BF16)
     row_copies = net.group()
-    for by in (2, 1, 3):
-        net.start("state", row_copies, row_tx, row_rx.at[z], z=step(z, by))
+    for later in (3, 2, 1):
+
+        @pl.when(z < later)
+        def _():
+            net.start(None, row_copies, row_tx, row_rx.at[z], z=later)
+
 
     u1b = two("up", "y", (up_own(1), up_at(z, y, 1)), (up_own(0), up_at(z, y, 0)))
     phase("s09b_w")
@@ -330,7 +336,8 @@
     phase("s10_waitrow")
 
     rdec_copies.wait()
-    row_copies.wait()
+    for earlier in range(1, 4):
+        pl.when(z == earlier)(lambda: row_copies.wait(earlier * bytes_of(row_tx)))
     phase("s11_incoming")
     run = jnp.zeros((QUARTER, DV), F32)
     for at in range(4):
@@ -582,14 +589,14 @@
     for d in (xm, xp):
         to_pair(d, 1, near[1])
     r0.work("xp", "xm")
-    phase("g0_wait_on")
-    arrived(on0)
-    to_pair(xo, 0, far[0])
     phase("g1_wait_pair")
     arrived(near[1])
     phase("m1_up_near")
     mix_up(xp, 1)
     mix_up(xm, 1)
+    phase("g0_wait_on")
+    arrived(on0)
+    to_pair(xo, 0, far[0])
     r0.send_b()
     r1.work("xp", "xm")
     phase("g0_wait_far")
@@ -604,8 +611,6 @@
     phase("m0_up_own")
     mix_up(x, 0)
     r0.send_a()
-    phase("m1_up_own")
-    mix_up(x, 1)
     phase("g1_wait_far")
     arrived(far[1])
     phase("m1_up_far")
@@ -613,14 +618,15 @@
     r1.work("xo")
     phase("w_wait_last")
     arrived(dn_last)
-    r2.work("xo")
+    r2.work("xo", "xp")
     r1.send_a()
-    r2.work("xp")
+    r2.work("xm")
     r2.send_a()
     r0.send_c()
-    r2.work("xm")
+    phase("m1_up_own")
+    mix_up(x, 1)
+    r2.send_b()
     r1.send_c()
-    r2.send_b()
     r0.work("x")
     r1.work("x")
     r2.work("x")
@@ -650,6 +656,9 @@
     phase("s35_finish")
     store.wait()
     net.finish()
+    for count in range(1, 4):
+        view = sized(count * bytes_of(row_tx))
+        pl.when(z == 3 - count)(lambda: pltpu.make_async_copy(view, view, send.at[N_SEND - 1]).wait())
     phase(None)
 
 

time: 85.5 us -> 81.5 us (0.953)
  Pallas kernels: 83.5 us -> 79.5 us
    pallas_call x1, Pallas kernels: 83.5 us -> 79.5 us  [body(): pl.pallas_call(kernel, out_shape=jax.ShapeDtypeStruct((128, D), BF16), in...]
where the time goes in v4:
time: 81.5 us; the launch traced here: 81.3 us
  Pallas kernels  79.5 us (98%)
  local copies, waits for them, and re-layouts  1.88 us (2%)
    pallas_call x1, Pallas kernels, body(): pl.pallas_call(kernel, out_shape=jax.ShapeDtypeStruct((128, D), BF16), in...  79.5 us
    unnamed x1, local copies, waits for them, and re-layouts  1.88 us

profile of v4, /device:TPU:1, one launch (start us, length us, event | category | flops | bytes accessed | tf_op | source)
XLA Modules:
  0.0 81.3 jit_solution(4270574738652634615)
XLA Ops:
  0.0 79.5 %shard_map.109 = bf16[128,2048]{1,0:T(8,128)(2,1)} custom-call(bf16[128,2048]{1,0:T(8,128)(2,1)} %resid.1, bf16[1024,256]{1,0:T(8,128)(2,1)} %q_in.1, bf16[1024,256]{1,0:T(8,128)(2,1)} %k_in.1, bf16[1024,512]{1,0:T(8,128)(2,1)} %v_in.1, bf16[1024,512]{1,0:T(8,128)(2,1)} %g_in.1, f32[8,128]{1,0:T(8,128)} %bitcast.1, bf16[512,2048]{1,0:T(8,128)(2,1)} %wo_in.1, ...), custom_call_target="tpu_custom_call" | custom-call | tf_op jit(solution)/shard_map/pallas_call | solution.py:692
  79.5 1.9 %copy.13 = bf16[128,2048]{1,0:T(8,128)(2,1)} copy(bf16[128,2048]{1,0:T(8,128)(2,1)} %shard_map.109) | data formatting | bytes 1048576
